TPU v7x, 32 devices: a whole 2x2x4 slice. The times are simulated.
32 devices in a mesh: sp: 4 (over z), dp: 8 (over y, x, core).
Axes of the slice: x: 2, y: 2, z: 4, core: 2. Of those that a mesh axis runs over, the one named last changes fastest.
Arguments:
- inputs: bfloat16 [8, 544, 2048], P('dp', 'sp'), may hold values from -6 to 6
- query_vectors: bfloat16 [8, 544, 1024], P('dp', 'sp'), may hold values from -6 to 6
- key_vectors: bfloat16 [8, 544, 1024], P('dp', 'sp'), may hold values from -6 to 6
- value_vectors: bfloat16 [8, 544, 1024], P('dp', 'sp'), may hold values from -6 to 6
- cotangent: bfloat16 [8, 544, 1024], P('dp', 'sp'), may hold values from -6 to 6
- gate_prefix: float32 [8, 16, 544], P('dp', 'sp'), may hold values from -544 to 0, as said below
- value_weight: bfloat16 [2048, 1024], P('sp', 'dp'), may hold values from -0.125 to 0.125
Outputs:
- query_grad: bfloat16 [8, 544, 1024], P('dp', 'sp')
- key_grad: bfloat16 [8, 544, 1024], P('dp', 'sp')
- input_grad: bfloat16 [8, 544, 2048], P('dp', 'sp')
- weight_grad: float32 [2048, 1024], P('sp', 'dp')
Inputs may be any that keep to these rules, and one draw needn't show every extreme that they name: `gate_prefix`: non-increasing along the positions of each sequence and head.
All inputs are finite; a program needn't handle non-finite values.
Results may differ from a plain program's by a relative error of at most 0.015.
Values may be sent and summed in bfloat16 or wider, within the bound.
A program may use at most 128 MiB of HBM per device.

v0:
```python
import functools

import jax
import jax.numpy as jnp
from jax import lax
from jax.experimental import pallas as pl
from jax.experimental.pallas import tpu as pltpu
from jax.sharding import PartitionSpec as P

HEAD_DIM = 64


def attention_backward(query_heads, key_heads, value_heads, grad_heads, prefix):
    length = query_heads.shape[0]
    score_scale = HEAD_DIM ** (-0.5)
    block_count = max(1, length // 512)
    block_rows = length // block_count
    key_accum = jnp.zeros(key_heads.shape, jnp.float32)
    value_accum = jnp.zeros(key_heads.shape, jnp.float32)
    query_parts = []
    for block_index in range(block_count):
        first_row = block_index * block_rows
        last_row = first_row + block_rows
        query_rows = query_heads[first_row:last_row]
        key_rows = key_heads[:last_row]
        grad_rows = grad_heads[first_row:last_row]
        scores = (
            jnp.einsum("qhd,khd->hqk", query_rows, key_rows, preferred_element_type=jnp.float32)
            * score_scale
        )
        scores = scores + prefix[:, first_row:last_row, None] - prefix[:, None, :last_row]
        causal = jnp.arange(last_row)[None, :] <= (first_row + jnp.arange(block_rows))[:, None]
        scores = jnp.where(causal[None], scores, -jnp.inf)
        row_peak = jnp.max(scores, axis=-1, keepdims=True)
        raised_scores = jnp.exp(scores - row_peak)
        softmax_rows = raised_scores / jnp.sum(raised_scores, axis=-1, keepdims=True)
        softmax_low = softmax_rows.astype(jnp.bfloat16)
        value_accum = value_accum.at[:last_row].add(
            jnp.einsum("hqk,qhd->khd", softmax_low, grad_rows, preferred_element_type=jnp.float32)
        )
        softmax_grad = jnp.einsum(
            "qhd,khd->hqk", grad_rows, value_heads[:last_row], preferred_element_type=jnp.float32
        )
        row_term = jnp.sum(softmax_rows * softmax_grad, axis=-1, keepdims=True)
        score_low = (softmax_rows * (softmax_grad - row_term)).astype(jnp.bfloat16)
        query_parts.append(
            (
                jnp.einsum("hqk,khd->qhd", score_low, key_rows, preferred_element_type=jnp.float32)
                * score_scale
            ).astype(jnp.bfloat16)
        )
        key_accum = key_accum.at[:last_row].add(
            jnp.einsum("hqk,qhd->khd", score_low, query_rows, preferred_element_type=jnp.float32)
        )
    query_grad = jnp.concatenate(query_parts, axis=0)
    key_grad = (key_accum * score_scale).astype(jnp.bfloat16)
    return (query_grad, key_grad, value_accum.astype(jnp.bfloat16))


def shards(inputs, query_vectors, key_vectors, value_vectors, cotangent, gate_prefix, value_weight):
    query_seq, key_seq, value_seq, grad_seq, input_cols = (
        lax.all_to_all(query_vectors[0], "sp", split_axis=1, concat_axis=0, tiled=True),
        lax.all_to_all(key_vectors[0], "sp", split_axis=1, concat_axis=0, tiled=True),
        lax.all_to_all(value_vectors[0], "sp", split_axis=1, concat_axis=0, tiled=True),
        lax.all_to_all(cotangent[0], "sp", split_axis=1, concat_axis=0, tiled=True),
        lax.all_to_all(inputs[0], "sp", split_axis=1, concat_axis=0, tiled=True),
    )
    length = query_seq.shape[0]
    local_width = query_seq.shape[1]
    head_shape = (length, local_width // HEAD_DIM, HEAD_DIM)
    query_heads, key_heads, value_heads = attention_backward(
        query_seq.reshape(head_shape),
        key_seq.reshape(head_shape),
        value_seq.reshape(head_shape),
        grad_seq.reshape(head_shape),
        gate_prefix[0],
    )
    query_flat = query_heads.reshape(length, local_width)
    key_flat = key_heads.reshape(length, local_width)
    value_flat = value_heads.reshape(length, local_width)
    value_all = lax.all_gather(value_flat, "sp", axis=1, tiled=True)
    weight_block = lax.all_gather(value_weight, "dp", axis=1, tiled=True)
    weight_rows = lax.psum_scatter(
        lax.dot_general(
            value_all, input_cols, (((0,), (0,)), ((), ())), preferred_element_type=jnp.float32
        ).astype(jnp.bfloat16),
        "dp",
        scatter_dimension=0,
        tiled=True,
    ).astype(jnp.float32)
    weight_grad = weight_rows.T
    query_back, key_back = (
        lax.all_to_all(query_flat, "sp", split_axis=0, concat_axis=1, tiled=True),
        lax.all_to_all(key_flat, "sp", split_axis=0, concat_axis=1, tiled=True),
    )
    column_grad = lax.dot_general(
        value_all, weight_block, (((1,), (1,)), ((), ())), preferred_element_type=jnp.float32
    ).astype(jnp.bfloat16)
    input_grad = lax.all_to_all(column_grad, "sp", split_axis=0, concat_axis=1, tiled=True)
    return (query_back[None], key_back[None], input_grad[None], weight_grad)


LANES = 128
MESH = pl.DeviceIdType.MESH


def one_kernel_fits(sp_count, dp_count, inputs, query, key, value, cotangent, gate, weight):
    rows, width = query.shape[1:]
    model = inputs.shape[2]
    return (
        dp_count == 8
        and width == dp_count * LANES
        and width % (sp_count * LANES) == 0
        and LANES == 2 * HEAD_DIM
        and rows % 8 == 0
        and model % (sp_count * LANES) == 0
        and model % (2 * LANES) == 0
        and sp_count % 2 == 0
        and rows * sp_count <= 1024
        and (dp_count * rows + width) * model <= 3 * 2**21
    )


def query_blocks(length):
    return [(first, min(first + 256, length)) for first in range(0, length, 256)]


def own_lanes(head, *arrays):
    lane = lax.broadcasted_iota(jnp.int32, arrays[0].shape, 1)
    own = (lane < HEAD_DIM) if head == 0 else (lane >= HEAD_DIM)
    return [jnp.where(own, x, 0.0).astype(jnp.bfloat16) for x in arrays]


def add_block(ref, value, seen):
    if seen:
        ref[:seen] += value[:seen]
    if seen < value.shape[0]:
        ref[seen : value.shape[0]] = value[seen:]


dot = functools.partial(lax.dot_general, preferred_element_type=jnp.float32)
BY_LANES = (((1,), (1,)), ((), ()))
BY_ROWS = (((0,), (0,)), ((), ()))
PLAIN = (((1,), (0,)), ((), ()))


def softmax_pair(q32, k32, g32, gate_rows, gate_columns, soft_refs, dv_ref):
    length = q32.shape[0]
    scale = HEAD_DIM ** (-0.5)
    q_all = q32.astype(jnp.bfloat16)
    for head in range(2):
        k_own, g_own = own_lanes(head, k32, g32)
        for first, last in query_blocks(length):
            size = last - first
            scores = dot(k_own[:last], q_all[first:last], BY_LANES) * scale
            scores = scores + gate_rows[head][:, first:last] - gate_columns[head][:last]
            key_pos = lax.broadcasted_iota(jnp.int32, (last, size), 0)
            query_pos = lax.broadcasted_iota(jnp.int32, (last, size), 1) + first
            scores = jnp.where(key_pos <= query_pos, scores, -jnp.inf)
            peak = jnp.max(scores, axis=0, keepdims=True)
            raised = jnp.exp(scores - peak)
            soft = raised * (1.0 / jnp.sum(raised, axis=0, keepdims=True))
            soft_refs[head][:last, first:last] = soft
            add_block(
                dv_ref, dot(soft.astype(jnp.bfloat16), g_own[first:last], PLAIN),
                first if head == 0 else last,
            )


def gradient_pair(q32, k32, v32, g32, soft_refs, dq_ref, dk_ref):
    length = q32.shape[0]
    scale = HEAD_DIM ** (-0.5)
    g_all = g32.astype(jnp.bfloat16)
    for head in range(2):
        q_own, k_own, v_own = own_lanes(head, q32, k32, v32)
        for first, last in query_blocks(length):
            soft = soft_refs[head][:last, first:last]
            soft_grad = dot(v_own[:last], g_all[first:last], BY_LANES)
            row_term = jnp.sum(soft * soft_grad, axis=0, keepdims=True)
            score_low = (soft * (soft_grad - row_term)).astype(jnp.bfloat16)
            add_block(
                dk_ref, dot(score_low, q_own[first:last], PLAIN) * scale,
                first if head == 0 else last,
            )
            dq = dot(score_low, k_own[:last], BY_ROWS) * scale
            if head == 0:
                dq_ref[first:last] = dq
            else:
                dq_ref[first:last] += dq


def kernel(
    n, groups, in_hbm, q_hbm, k_hbm, v_hbm, g_hbm, gate_ref, w_hbm,
    qg_ref, kg_ref, ig_ref, wg_ref,
    in_ref, q_ref, k_ref, v_ref, g_ref, w_ref,
    pair_in, pair_out, vg, vg_seq, x_all, w_all, part, part_in, gate_pad, gate_t,
    soft, dq_ref, dk_ref, dv_ref, local_sems, hop_sems, hop_recv_sems, send_sems, recv_sems,
):
    s = lax.axis_index("sp")
    d = lax.axis_index("dp")
    core, x, y = d % 2, (d // 2) % 2, d // 4
    rows = q_ref.shape[0]
    length = n * rows
    half = in_ref.shape[1] // 2

    fetched = [
        pltpu.make_async_copy(src, dst, local_sems.at[i])
        for i, (src, dst) in enumerate(
            ((w_hbm, w_ref), (q_hbm, q_ref), (k_hbm, k_ref), (g_hbm, g_ref), (in_hbm, in_ref), (v_hbm, v_ref))
        )
    ]
    for copy in fetched:
        copy.start()

    def near(step):
        return (
            d
            + (step % 2) * (1 - 2 * core)
            + ((step // 2) % 2) * (2 - 4 * x)
            + (step // 4) * (4 - 8 * y)
        )

    partner, x_near, y_near, corner = near(1), near(2), near(4), near(6)
    started = []

    def send(src, dst, to_sp, to_dp):
        index = len(started)
        copy = pltpu.make_async_remote_copy(
            src_ref=src,
            dst_ref=dst,
            send_sem=send_sems.at[index],
            recv_sem=recv_sems.at[index],
            device_id={"sp": to_sp, "dp": to_dp},
            device_id_type=MESH,
        )
        copy.start()
        started.append(copy)
        return copy

    def lanes_of(device, p):
        return pl.ds(pl.multiple_of((device * groups + p) * LANES, LANES), LANES)

    barrier = pltpu.get_barrier_semaphore()
    for r in range(1, n):
        pl.semaphore_signal(barrier, inc=1, device_id={"sp": (s + r) % n, "dp": d}, device_id_type=MESH)
    for step in range(1, 8):
        pl.semaphore_signal(barrier, inc=1, device_id={"sp": s, "dp": near(step)}, device_id_type=MESH)
    pl.semaphore_wait(barrier, n - 1 + 7)
    for copy in fetched:
        copy.wait()

    def hop(t, up):
        block = (s - t + 1 + n) % n if up else (s + t - 1) % n
        src = w_ref if t == 1 else w_all.at[d, block]
        index = 2 * (t - 1) + int(up)
        return pltpu.make_async_remote_copy(
            src_ref=src,
            dst_ref=w_all.at[d, block],
            send_sem=hop_sems.at[index],
            recv_sem=hop_recv_sems.at[index],
            device_id={"sp": (s + 1) % n if up else (s - 1 + n) % n, "dp": d},
            device_id_type=MESH,
        )

    def hop_sends(t, act):
        pl.when((s >= t - 1) & (s < n - 1))(lambda: act(hop(t, True)))
        pl.when((s <= n - t) & (s > 0))(lambda: act(hop(t, False)))

    def hop_start(t):
        hop_sends(t, lambda copy: copy.start())

    def hop_arrive(t):
        pl.when(s >= t)(lambda: hop(t, True).wait_recv())
        pl.when(s < n - t)(lambda: hop(t, False).wait_recv())

    def send_pair(p, a, ref):
        return [
            send(ref.at[:, lanes_of((s + r) % n, p)], pair_in.at[p, a, s], (s + r) % n, d)
            for r in range(1, n)
        ]

    hop_start(1)
    early = [[] for _ in range(groups)]
    queue = [(p, a, ref) for p in range(groups) for a, ref in ((0, q_ref), (1, k_ref), (3, g_ref))]

    def send_early(count):
        for p, a, ref in queue[:count]:
            early[p].extend(send_pair(p, a, ref))
        del queue[:count]

    send_early(2)
    x_near0 = send(in_ref, x_all.at[d], s, x_near)
    y_near0 = send(in_ref, x_all.at[d], s, y_near)
    x_part0 = send(in_ref, x_all.at[d], s, partner)

    for p in range(groups):
        for a, ref in enumerate((q_ref, k_ref, v_ref, g_ref)):
            pair_in[p, a, s] = ref[:, lanes_of(s, p)]
    x_all[d] = in_ref[...]
    w_all[d, s] = w_ref[...]
    gate_pad[...] = jnp.zeros_like(gate_pad)
    gate_pad[: gate_ref.shape[0], :length] = gate_ref[...]
    gate_t[...] = gate_pad[...].T

    def wide(p, a):
        return pair_in[p, a].astype(jnp.float32).reshape(length, LANES)

    def give_back(p, a, ref):
        pair_out[p, a] = ref[...].reshape(n, rows, LANES).astype(jnp.bfloat16)
        copies = []
        for r in range(1, n):
            to = (s + r) % n
            dst = (
                vg.at[s * groups + p] if a == 0
                else (None, qg_ref, kg_ref)[a].at[:, lanes_of(s, p)]
            )
            copies.append(send(pair_out.at[p, a, to], dst, to, d))
        return copies

    def first_half(p):
        for copy in early[p]:
            copy.wait_recv()

    def softmax_part(p):
        heads = (2 * p, 2 * p + 1)
        softmax_pair(
            wide(p, 0), wide(p, 1), wide(p, 3),
            [gate_pad[h : h + 1, :length] for h in heads],
            [gate_t[:length, h : h + 1] for h in heads],
            [soft.at[h] for h in heads],
            dv_ref,
        )
        copies = give_back(p, 0, dv_ref)
        vg[s * groups + p] = pair_out[p, 0, s]
        return copies

    def gradient_part(p):
        gradient_pair(
            wide(p, 0), wide(p, 1), wide(p, 2), wide(p, 3),
            [soft.at[2 * p], soft.at[2 * p + 1]], dq_ref, dk_ref,
        )
        copies = give_back(p, 1, dq_ref) + give_back(p, 2, dk_ref)
        qg_ref[:, lanes_of(s, p)] = pair_out[p, 1, s]
        kg_ref[:, lanes_of(s, p)] = pair_out[p, 2, s]
        return copies

    def spread_middle(buffer, low, high, from_x, from_y):
        from_x.wait_recv()
        a = send(low(x_near), low(x_near), s, y_near)
        b = send(buffer.at[x_near], buffer.at[x_near], s, partner)
        from_y.wait_recv()
        c = send(high(y_near), high(y_near), s, x_near)
        e = send(buffer.at[y_near], buffer.at[y_near], s, partner)
        return a, c, b, e

    def spread_last(buffer, middle):
        middle[0].wait_recv()
        middle[1].wait_recv()
        return send(buffer.at[corner], buffer.at[corner], s, partner)

    x_low = lambda i: x_all.at[i, :, pl.ds(0, half)]
    x_high = lambda i: x_all.at[i, :, pl.ds(half, half)]
    w_low = lambda i: w_all.at[i, pl.ds(0, n // 2)]
    w_high = lambda i: w_all.at[i, pl.ds(n // 2, n // 2)]

    back_v, back_qk, late = [], [], []
    x_middle = None
    hop_next = 1

    def relay():
        nonlocal hop_next
        if hop_next < n:
            hop_arrive(hop_next)
            if hop_next + 1 < n:
                hop_start(hop_next + 1)
            hop_next += 1

    relay()
    send_early(2)
    relay()
    send_early(len(queue))
    x_middle = spread_middle(x_all, x_low, x_high, x_near0, y_near0)
    for p in range(groups):
        if p == groups - 1:
            while hop_next < n:
                relay()
            w_x = send(w_all.at[d], w_all.at[d], s, x_near)
            w_y = send(w_all.at[d], w_all.at[d], s, y_near)
            w_part = send(w_all.at[d], w_all.at[d], s, partner)
            x_last = spread_last(x_all, x_middle)
        first_half(p)
        back_v += softmax_part(p)
        late.append(send_pair(p, 2, v_ref))

    for p in range(groups - 1):
        for copy in late[p]:
            copy.wait_recv()
        back_qk += gradient_part(p)

    for copy in back_v:
        copy.wait_recv()
    moved = [send(vg.at[near(step)], vg_seq.at[d], s, near(step)) for step in range(1, 8)]
    vg_seq[d] = vg[d]
    w_middle = spread_middle(w_all, w_low, w_high, w_x, w_y)
    for copy in late[groups - 1]:
        copy.wait_recv()
    back_qk += gradient_part(groups - 1)
    for copy in (x_part0, x_middle[2], x_middle[3], x_last):
        copy.wait_recv()
    for copy in moved:
        copy.wait_recv()

    block = in_ref.shape[1] // n
    def weight_part(j):
        columns = pl.ds(pl.multiple_of(j * block, LANES), block)
        total = None
        for i in range(8):
            term = dot(vg_seq[i], x_all[i, :, columns], BY_ROWS)
            total = term if total is None else total + term
        return total

    def send_part(j, slot, to):
        return send(part.at[j], part_in.at[slot], to, d)

    two_steps = n == 4
    if two_steps:
        mate, across = s + 1 - 2 * (s % 2), (s + 2) % n
        far = (mate + 2) % n
        part[far] = weight_part(far).astype(jnp.bfloat16)
        far_sum = send_part(far, 0, mate)
        part[mate] = weight_part(mate).astype(jnp.bfloat16)
        sums = [send_part(mate, 1, mate)]
        across_sum = weight_part(across)
        own_sum = weight_part(s)
        w_last = spread_last(w_all, w_middle)
        far_sum.wait_recv()
        part[across] = (across_sum + part_in[0].astype(jnp.float32)).astype(jnp.bfloat16)
        sums.append(send_part(across, 2, across))
    else:
        sums = []
        for r in range(1, n):
            to = (s + r) % n
            part[to] = weight_part(to).astype(jnp.bfloat16)
            sums.append(send_part(to, r - 1, to))
        own_sum = weight_part(s)
        w_last = spread_last(w_all, w_middle)
    first_slot = int(two_steps)

    for copy in (w_part, w_middle[2], w_middle[3], w_last):
        copy.wait_recv()
    vg_rows = jnp.concatenate([vg[i] for i in range(8)], axis=1)
    for j in range(n):
        w_rows = jnp.concatenate([w_all[i, j] for i in range(8)], axis=1)
        ig_ref[:, j * block : (j + 1) * block] = dot(vg_rows, w_rows, BY_LANES).astype(jnp.bfloat16)

    for copy in back_qk:
        copy.wait_recv()
    for copy in started:
        if all(copy is not other for other in sums):
            copy.wait_send()
    for t in range(1, n):
        hop_sends(t, lambda copy: copy.wait_send())
    total = own_sum
    for r, copy in enumerate(sums):
        copy.wait_recv()
        total = total + part_in[first_slot + r].astype(jnp.float32)
    wg_ref[...] = total.T
    for copy in sums:
        copy.wait_send()


def put_out(*refs):
    sems = refs[-1]
    copies = [pltpu.make_async_copy(refs[i], refs[4 + i], sems.at[i]) for i in range(4)]
    for copy in copies:
        copy.start()
    for copy in copies:
        copy.wait()


def fused(mesh, inputs, query, key, value, cotangent, gate, weight):
    n = mesh.shape["sp"]
    rows, width = query.shape[1:]
    model = inputs.shape[2]
    groups = width // (n * LANES)
    length = n * rows
    padded = -(-length // LANES) * LANES
    bf16, f32 = jnp.bfloat16, jnp.float32
    copies = (n - 1) * (7 * groups + 1) + 2 * 8 + 7
    vmem = pl.BlockSpec(memory_space=pltpu.VMEM)
    hbm = pl.BlockSpec(memory_space=pl.ANY)
    results = (
        jax.ShapeDtypeStruct((rows, width), bf16),
        jax.ShapeDtypeStruct((rows, width), bf16),
        jax.ShapeDtypeStruct((rows, model), bf16),
        jax.ShapeDtypeStruct((model // n, LANES), f32),
    )
    outs = pl.pallas_call(
        functools.partial(kernel, n, groups),
        out_shape=tuple(pltpu.VMEM(x.shape, x.dtype) for x in results),
        in_specs=[hbm] * 5 + [vmem, hbm],
        out_specs=(vmem,) * 4,
        scratch_shapes=[
            pltpu.VMEM((rows, model), bf16),
            *[pltpu.VMEM((rows, width), bf16)] * 4,
            pltpu.VMEM((model // n, LANES), bf16),
            pltpu.VMEM((groups, 4, n, rows, LANES), bf16),
            pltpu.VMEM((groups, 3, n, rows, LANES), bf16),
            pltpu.VMEM((8, rows, LANES), bf16),
            pltpu.VMEM((8, rows, LANES), bf16),
            pltpu.VMEM((8, rows, model), bf16),
            pltpu.VMEM((8, n, model // n, LANES), bf16),
            pltpu.VMEM((n, LANES, model // n), bf16),
            pltpu.VMEM((n - 1, LANES, model // n), bf16),
            pltpu.VMEM((LANES, padded), f32),
            pltpu.VMEM((padded, LANES), f32),
            pltpu.VMEM((2 * groups, length, length), f32),
            *[pltpu.VMEM((length, LANES), f32)] * 3,
            pltpu.SemaphoreType.DMA((6,)),
            *[pltpu.SemaphoreType.DMA((2 * (n - 1),))] * 2,
            pltpu.SemaphoreType.DMA((copies,)),
            pltpu.SemaphoreType.DMA((copies,)),
        ],
        compiler_params=pltpu.CompilerParams(
            collective_id=0, has_side_effects=True, vmem_limit_bytes=60 * 2**20
        ),
    )(inputs[0], query[0], key[0], value[0], cotangent[0], gate[0], weight)
    query_grad, key_grad, input_grad, weight_grad = pl.pallas_call(
        put_out,
        out_shape=results,
        in_specs=[vmem] * 4,
        out_specs=(hbm,) * 4,
        scratch_shapes=[pltpu.SemaphoreType.DMA((4,))],
        compiler_params=pltpu.CompilerParams(vmem_limit_bytes=2**20),
    )(*(pltpu.with_memory_space_constraint(x, pltpu.VMEM) for x in outs))
    return (query_grad[None], key_grad[None], input_grad[None], weight_grad)


def solution(mesh):
    in_specs = (
        P("dp", "sp", None),
        P("dp", "sp", None),
        P("dp", "sp", None),
        P("dp", "sp", None),
        P("dp", "sp", None),
        P("dp", "sp", None),
        P("sp", "dp"),
    )
    out_specs = (P("dp", "sp", None), P("dp", "sp", None), P("dp", "sp", None), P("sp", "dp"))
    sp_count, dp_count = mesh.shape["sp"], mesh.shape["dp"]

    def per_device(*arrays):
        if one_kernel_fits(sp_count, dp_count, *arrays):
            return fused(mesh, *arrays)
        return shards(*arrays)

    return jax.shard_map(per_device, mesh=mesh, in_specs=in_specs, out_specs=out_specs, check_vma=False)
```

profile of v0, /device:TPU:1, one launch (start us, length us, event | category | flops | bytes accessed | tf_op | source)
XLA Modules:
  0.0 64.3 jit_solution(12219397840626551692)
XLA Ops:
  0.6 62.6 %shard_map.102 = (bf16[136,1024]{1,0:T(8,128)(2,1)S(1)}, bf16[136,1024]{1,0:T(8,128)(2,1)S(1)}, bf16[136,2048]{1,0:T(8,128)(2,1)S(1)}, f32[512,128]{1,0:T(8,128)S(1)}) custom-call(bf16[136,2048]{1,0:T(8,128)(2,1)} %bitcast.9, bf16[136,1024]{1,0:T(8,128)(2,1)} %bitcast.10, bf16[136,1024]{1,0:T(8,128)(2,1)} %bitcast.11, bf16[136,1024]{1,0:T(8,128)(2,1)} %bitcast.12, ...), custom_call_target="tpu_custom_call" | custom-call | tf_op jit(solution)/shard_map/pallas_call | solution.py:498
  63.2 1.1 %shard_map.103 = (bf16[136,1024]{1,0:T(8,128)(2,1)}, bf16[136,1024]{1,0:T(8,128)(2,1)}, bf16[136,2048]{1,0:T(8,128)(2,1)}, f32[512,128]{1,0:T(8,128)}) custom-call(bf16[136,1024]{1,0:T(8,128)(2,1)S(1)} %get-tuple-element.12.refs_0_, bf16[136,1024]{1,0:T(8,128)(2,1)S(1)} %get-tuple-element.13.refs_1_, bf16[136,2048]{1,0:T(8,128)(2,1)S(1)} %get-tuple-element.14.refs_2_, ...), custom_call_target="tpu_custom_call" | custom-call | tf_op jit(solution)/shard_map/pallas_call | solution.py:528
where the time goes:
time: 65.1 us; the launch traced here: 64.3 us
  Pallas kernels  63.7 us (98%)
    pallas_call x1, Pallas kernels, fused(): pl.pallas_call(functools.partial(kernel, n, groups), out_shape=tuple((plt...  62.6 us

commit v1 on v0

v1 whole, which is shorter than its diff:
```python
import functools

import jax
import jax.numpy as jnp
from jax import lax
from jax.experimental import pallas as pl
from jax.experimental.pallas import tpu as pltpu
from jax.sharding import PartitionSpec as P

HEAD_DIM = 64


def attention_backward(query_heads, key_heads, value_heads, grad_heads, prefix):
    length = query_heads.shape[0]
    score_scale = HEAD_DIM ** (-0.5)
    block_count = max(1, length // 512)
    block_rows = length // block_count
    key_accum = jnp.zeros(key_heads.shape, jnp.float32)
    value_accum = jnp.zeros(key_heads.shape, jnp.float32)
    query_parts = []
    for block_index in range(block_count):
        first_row = block_index * block_rows
        last_row = first_row + block_rows
        query_rows = query_heads[first_row:last_row]
        key_rows = key_heads[:last_row]
        grad_rows = grad_heads[first_row:last_row]
        scores = (
            jnp.einsum("qhd,khd->hqk", query_rows, key_rows, preferred_element_type=jnp.float32)
            * score_scale
        )
        scores = scores + prefix[:, first_row:last_row, None] - prefix[:, None, :last_row]
        causal = jnp.arange(last_row)[None, :] <= (first_row + jnp.arange(block_rows))[:, None]
        scores = jnp.where(causal[None], scores, -jnp.inf)
        row_peak = jnp.max(scores, axis=-1, keepdims=True)
        raised_scores = jnp.exp(scores - row_peak)
        softmax_rows = raised_scores / jnp.sum(raised_scores, axis=-1, keepdims=True)
        softmax_low = softmax_rows.astype(jnp.bfloat16)
        value_accum = value_accum.at[:last_row].add(
            jnp.einsum("hqk,qhd->khd", softmax_low, grad_rows, preferred_element_type=jnp.float32)
        )
        softmax_grad = jnp.einsum(
            "qhd,khd->hqk", grad_rows, value_heads[:last_row], preferred_element_type=jnp.float32
        )
        row_term = jnp.sum(softmax_rows * softmax_grad, axis=-1, keepdims=True)
        score_low = (softmax_rows * (softmax_grad - row_term)).astype(jnp.bfloat16)
        query_parts.append(
            (
                jnp.einsum("hqk,khd->qhd", score_low, key_rows, preferred_element_type=jnp.float32)
                * score_scale
            ).astype(jnp.bfloat16)
        )
        key_accum = key_accum.at[:last_row].add(
            jnp.einsum("hqk,qhd->khd", score_low, query_rows, preferred_element_type=jnp.float32)
        )
    query_grad = jnp.concatenate(query_parts, axis=0)
    key_grad = (key_accum * score_scale).astype(jnp.bfloat16)
    return (query_grad, key_grad, value_accum.astype(jnp.bfloat16))


def shards(inputs, query_vectors, key_vectors, value_vectors, cotangent, gate_prefix, value_weight):
    query_seq, key_seq, value_seq, grad_seq, input_cols = (
        lax.all_to_all(query_vectors[0], "sp", split_axis=1, concat_axis=0, tiled=True),
        lax.all_to_all(key_vectors[0], "sp", split_axis=1, concat_axis=0, tiled=True),
        lax.all_to_all(value_vectors[0], "sp", split_axis=1, concat_axis=0, tiled=True),
        lax.all_to_all(cotangent[0], "sp", split_axis=1, concat_axis=0, tiled=True),
        lax.all_to_all(inputs[0], "sp", split_axis=1, concat_axis=0, tiled=True),
    )
    length = query_seq.shape[0]
    local_width = query_seq.shape[1]
    head_shape = (length, local_width // HEAD_DIM, HEAD_DIM)
    query_heads, key_heads, value_heads = attention_backward(
        query_seq.reshape(head_shape),
        key_seq.reshape(head_shape),
        value_seq.reshape(head_shape),
        grad_seq.reshape(head_shape),
        gate_prefix[0],
    )
    query_flat = query_heads.reshape(length, local_width)
    key_flat = key_heads.reshape(length, local_width)
    value_flat = value_heads.reshape(length, local_width)
    value_all = lax.all_gather(value_flat, "sp", axis=1, tiled=True)
    weight_block = lax.all_gather(value_weight, "dp", axis=1, tiled=True)
    weight_rows = lax.psum_scatter(
        lax.dot_general(
            value_all, input_cols, (((0,), (0,)), ((), ())), preferred_element_type=jnp.float32
        ).astype(jnp.bfloat16),
        "dp",
        scatter_dimension=0,
        tiled=True,
    ).astype(jnp.float32)
    weight_grad = weight_rows.T
    query_back, key_back = (
        lax.all_to_all(query_flat, "sp", split_axis=0, concat_axis=1, tiled=True),
        lax.all_to_all(key_flat, "sp", split_axis=0, concat_axis=1, tiled=True),
    )
    column_grad = lax.dot_general(
        value_all, weight_block, (((1,), (1,)), ((), ())), preferred_element_type=jnp.float32
    ).astype(jnp.bfloat16)
    input_grad = lax.all_to_all(column_grad, "sp", split_axis=0, concat_axis=1, tiled=True)
    return (query_back[None], key_back[None], input_grad[None], weight_grad)


LANES = 128
MESH = pl.DeviceIdType.MESH


def one_kernel_fits(sp_count, dp_count, inputs, query, key, value, cotangent, gate, weight):
    rows, width = query.shape[1:]
    model = inputs.shape[2]
    return (
        dp_count == 8
        and width == dp_count * LANES
        and width % (sp_count * LANES) == 0
        and gate.shape[1] * sp_count * HEAD_DIM == width
        and gate.shape[2] == rows * sp_count
        and LANES == 2 * HEAD_DIM
        and rows % 8 == 0
        and model % (sp_count * LANES) == 0
        and model % (2 * LANES) == 0
        and sp_count == 4
        and rows * sp_count <= 1024
        and (dp_count * rows + width) * model <= 3 * 2**21
    )


dot = functools.partial(lax.dot_general, preferred_element_type=jnp.float32)
BY_LANES = (((1,), (1,)), ((), ()))
BY_ROWS = (((0,), (0,)), ((), ()))
PLAIN = (((1,), (0,)), ((), ()))
LOWEST = -1e30


def own_lanes(head, *arrays):
    lane = lax.broadcasted_iota(jnp.int32, arrays[0].shape, 1)
    own = (lane < HEAD_DIM) if head == 0 else (lane >= HEAD_DIM)
    return [jnp.where(own, x, 0.0).astype(jnp.bfloat16) for x in arrays]


def lanes(p):
    return pl.ds(p * LANES if isinstance(p, int) else pl.multiple_of(p * LANES, LANES), LANES)


def padded(columns):
    return -(-columns // LANES) * LANES


def plus(total, term):
    return term if total is None else total + term


def causal(scores, rows, keys_first):
    columns = scores.shape[1]
    start = columns - rows
    low = start // LANES * LANES
    tail = scores[:, low:]
    row = lax.broadcasted_iota(jnp.int32, tail.shape, 0)
    column = lax.broadcasted_iota(jnp.int32, tail.shape, 1) + (low - start)
    kept = ((column >= row) | (column < 0)) if keys_first else (column <= row)
    tail = jnp.where(kept, tail, -jnp.inf)
    return jnp.concatenate([scores[:, :low], tail], axis=1) if low else tail


def kernel(
    n, half, in_hbm, q_hbm, k_hbm, v_hbm, g_hbm, gate_ref, w_hbm,
    qg_ref, kg_ref, ig_ref, wg_ref,
    in_ref, q_ref, k_ref, v_ref, g_ref, w_ref,
    kv_in, qg_in, down_in, down_out, up_in, up_out, down_acc, up_acc,
    vg, vg_seq, x_all, w_all, part, part_in, sum_ref,
    gate_all, gate_pad, gate_t, gate_rev, soft, raised, value_dot,
    peaks, factors, row_terms, stats,
    local_sems, send_sems, recv_sems,
):
    s = lax.axis_index("sp")
    d = lax.axis_index("dp")
    core, x, y = d % 2, (d // 2) % 2, d // 4
    rows, model = in_ref.shape
    last = n - 1
    low, high = pl.ds(0, model // 2), pl.ds(model // 2, model // 2)
    block = model // n
    scale = HEAD_DIM ** (-0.5)
    f32, bf16 = jnp.float32, jnp.bfloat16

    fetched = [
        pltpu.make_async_copy(src, dst, local_sems.at[i])
        for i, (src, dst) in enumerate(
            ((k_hbm, k_ref), (q_hbm, q_ref), (in_hbm, in_ref), (w_hbm, w_ref), (v_hbm, v_ref), (g_hbm, g_ref))
        )
    ]
    for copy in fetched:
        copy.start()

    def near(step):
        return (
            d
            + (step % 2) * (1 - 2 * core)
            + ((step // 2) % 2) * (2 - 4 * x)
            + (step // 4) * (4 - 8 * y)
        )

    partner, x_near, y_near, corner = near(1), near(2), near(4), near(6)

    ids = {}
    used = [0]

    def sem(key, count=1):
        if key not in ids:
            ids[key] = used[0]
            used[0] += count
            assert used[0] <= send_sems.shape[0]
        return ids[key]

    def remote(src, dst, send_id, recv_id, to_sp, to_dp):
        return pltpu.make_async_remote_copy(
            src_ref=src,
            dst_ref=dst,
            send_sem=send_sems.at[send_id],
            recv_sem=recv_sems.at[recv_id],
            device_id={"sp": to_sp, "dp": to_dp},
            device_id_type=MESH,
        )

    def named(name, src, dst, to_sp, to_dp):
        i = sem(name)
        return remote(src, dst, i, i, to_sp, to_dp)

    def up(si, a, b, p):
        src = (k_ref, v_ref)[a].at[:, lanes(p)] if b == si else kv_in.at[a, p, b]
        i = sem(("up", a, b), half) + p
        return remote(src, kv_in.at[a, p, b], i, i, s + 1, d)

    def up_arrive(a, b, p):
        i = sem(("up", a, b), half) + p
        remote(kv_in.at[a, p, b], kv_in.at[a, p, b], i, i, (s + 1) % n, d).wait_recv()

    def down(si, a, b, p):
        src = (q_ref, g_ref)[a].at[:, lanes(half + p)] if b == si else qg_in.at[a, p, last - b]
        i = sem(("down", a, b), half) + p
        return remote(src, qg_in.at[a, p, last - b], i, i, s - 1, d)

    def down_arrive(a, b, p):
        i = sem(("down", a, b), half) + p
        remote(qg_in.at[a, p, last - b], qg_in.at[a, p, last - b], i, i, (s + 1) % n, d).wait_recv()

    def down_sum(c, b, p):
        i = sem(("down sum", c, b), half) + p
        return remote(down_out.at[c, p, b], down_in.at[c, p, b], i, i, (s + n - 1) % n, d)

    def up_sum(j, p):
        i = sem(("up sum", j), half) + p
        return remote(up_out.at[p, j], up_in.at[p, j], i, i, (s + 1) % n, d)

    def gate_copy(sender, to):
        i = sem("gate", n)
        return remote(gate_ref, gate_all.at[sender], i + to, i + sender, to, d)

    def stat_width(a, b):
        return padded(rows * (n - max(a, b)))

    def stat_copy(which, sender, to):
        i = sem(("stat", which), n)
        piece = stats.at[which, sender, :, pl.ds(0, stat_width(sender, to))]
        return remote(piece, piece, i + to, i + sender, to, d)

    def hop(si, b, upward):
        src = w_ref if b == si else w_all.at[d, b]
        i = sem(("hop", upward), n) + b
        return remote(src, w_all.at[d, b], i, i, (s + 1) % n if upward else (s + n - 1) % n, d)

    def vg_copy(p):
        i = sem("vg", 2 * half)
        return remote(vg.at[p], vg_seq.at[d], i + p, i + d, s, p)

    def send_vg(p):
        @pl.when(d != p)
        def _():
            vg_copy(p).start()

        @pl.when(d == p)
        def _():
            vg_seq[p] = vg[p]

    def x_copy(name):
        return {
            "x low": lambda: named(name, in_ref.at[:, low], x_all.at[d, :, low], s, x_near),
            "x high": lambda: named(name, in_ref.at[:, high], x_all.at[d, :, high], s, x_near),
            "y high": lambda: named(name, in_ref.at[:, high], x_all.at[d, :, high], s, y_near),
            "y low": lambda: named(name, in_ref.at[:, low], x_all.at[d, :, low], s, y_near),
            "own": lambda: named(name, in_ref, x_all.at[d], s, partner),
            "on y": lambda: named(name, x_all.at[x_near, :, low], x_all.at[x_near, :, low], s, y_near),
            "on x": lambda: named(name, x_all.at[y_near, :, high], x_all.at[y_near, :, high], s, x_near),
            "x over": lambda: named(name, x_all.at[x_near], x_all.at[x_near], s, partner),
            "y over": lambda: named(name, x_all.at[y_near], x_all.at[y_near], s, partner),
            "corner over": lambda: named(name, x_all.at[corner], x_all.at[corner], s, partner),
        }[name]()

    x_start = ("x low", "y high", "x high", "y low", "own")
    x_rest = ("on y", "on x", "x over", "y over", "corner over")

    def x_middle():
        x_copy("x low").wait_recv()
        x_copy("on y").start()
        x_copy("y high").wait_recv()
        x_copy("on x").start()
        x_copy("x high").wait_recv()
        x_copy("x over").start()
        x_copy("y low").wait_recv()
        x_copy("y over").start()

    def x_last():
        x_copy("on y").wait_recv()
        x_copy("on x").wait_recv()
        x_copy("corner over").start()

    w_lower, w_upper = pl.ds(0, block // 2), pl.ds(block // 2, block // 2)

    def w_copy(name, j, own=False):
        src = w_ref if own else w_all.at[d, j]
        key = ("w", name, j)
        return {
            "x": lambda: named(key, src, w_all.at[d, j], s, x_near),
            "y": lambda: named(key, src, w_all.at[d, j], s, y_near),
            "own": lambda: named(key, src, w_all.at[d, j], s, partner),
            "on y": lambda: named(key, w_all.at[x_near, j, w_lower], w_all.at[x_near, j, w_lower], s, y_near),
            "on x": lambda: named(key, w_all.at[y_near, j, w_upper], w_all.at[y_near, j, w_upper], s, x_near),
            "x over": lambda: named(key, w_all.at[x_near, j], w_all.at[x_near, j], s, partner),
            "y over": lambda: named(key, w_all.at[y_near, j], w_all.at[y_near, j], s, partner),
            "corner over": lambda: named(key, w_all.at[corner, j], w_all.at[corner, j], s, partner),
        }[name]()

    w_names = ("x", "y", "own", "on y", "on x", "x over", "y over", "corner over")

    def w_start(j, own=False):
        for name in ("x", "y", "own"):
            w_copy(name, j, own).start()

    def w_middle(j):
        w_copy("x", j).wait_recv()
        w_copy("on y", j).start()
        w_copy("y", j).wait_recv()
        w_copy("on x", j).start()
        w_copy("x over", j).start()
        w_copy("y over", j).start()

    def w_last(j):
        w_copy("on y", j).wait_recv()
        w_copy("on x", j).wait_recv()
        w_copy("corner over", j).start()

    def wide(buffer, a, p, count):
        return buffer[a, p, :count].astype(f32).reshape(count * rows, LANES)

    def own32(ref, p):
        return ref[:, lanes(p)].astype(f32)

    def gate_column(si, head):
        own = gate_t[rows * si : rows * si + rows]
        lane = lax.broadcasted_iota(jnp.int32, own.shape, 1)
        return jnp.sum(jnp.where(lane == head, own, 0.0), axis=1, keepdims=True)

    def softmax_queries(si, p):
        columns = rows * (si + 1)
        q32, g32 = own32(q_ref, p), own32(g_ref, p)
        keys = wide(kv_in, 0, p, si + 1).astype(bf16)
        total = None
        for h in range(2):
            head = 2 * p + h
            q_own, g_own = own_lanes(h, q32, g32)
            scores = dot(q_own, keys, BY_LANES) * scale
            scores = scores + gate_column(si, head) - gate_pad[pl.ds(head, 1), :columns]
            scores = causal(scores, rows, False)
            peak = jnp.max(scores, axis=1, keepdims=True)
            up_scores = jnp.exp(scores - peak)
            part_soft = up_scores * (1.0 / jnp.sum(up_scores, axis=1, keepdims=True))
            soft[head, :, :columns] = part_soft
            total = plus(total, dot(part_soft.astype(bf16), g_own, BY_ROWS))
        return total

    def gradient_queries(si, p):
        columns = rows * (si + 1)
        q32, g32 = own32(q_ref, p), own32(g_ref, p)
        keys32 = wide(kv_in, 0, p, si + 1)
        values = wide(kv_in, 1, p, si + 1).astype(bf16)
        dq = dk = None
        for h in range(2):
            q_own, g_own = own_lanes(h, q32, g32)
            (k_own,) = own_lanes(h, keys32)
            part_soft = soft[2 * p + h, :, :columns]
            soft_grad = dot(g_own, values, BY_LANES)
            row_term = jnp.sum(part_soft * soft_grad, axis=1, keepdims=True)
            score_low = (part_soft * (soft_grad - row_term)).astype(bf16)
            dq = plus(dq, dot(score_low, k_own, PLAIN))
            dk = plus(dk, dot(score_low, q_own, BY_ROWS))
        qg_ref[:, lanes(p)] = (dq * scale).astype(bf16)
        return dk * scale

    def softmax_keys(si, p):
        columns = rows * (n - si)
        k32 = own32(k_ref, half + p)
        queries = wide(qg_in, 0, p, n - si).astype(bf16)
        for h in range(2):
            row = 2 * p + h
            head = 2 * half + row
            (k_own,) = own_lanes(h, k32)
            scores = dot(k_own, queries, BY_LANES) * scale
            scores = scores + gate_rev[pl.ds(head, 1), :columns] - gate_column(si, head)
            scores = causal(scores, rows, True)
            peak = jnp.max(scores, axis=0, keepdims=True)
            up_scores = jnp.exp(scores - peak)
            raised[row, :, :columns] = up_scores
            peaks[pl.ds(row, 1), :columns] = peak
            stats[0, si, pl.ds(row, 1), :columns] = peak + jnp.log(
                jnp.sum(up_scores, axis=0, keepdims=True)
            )

    def stat_pieces(si, which, empty):
        width = padded(rows * (n - si))
        pieces = []
        for u in range(n):
            held = stat_width(si, u)
            piece = stats[which, u, :, :held]
            lane = lax.broadcasted_iota(jnp.int32, piece.shape, 1)
            piece = jnp.where(lane < rows * (n - u), piece, empty)
            if held < width:
                rest = jnp.full((piece.shape[0], width - held), empty, f32)
                piece = jnp.concatenate([piece, rest], axis=1)
            pieces.append(piece)
        return pieces, width

    def join_peaks(si):
        pieces, width = stat_pieces(si, 0, LOWEST)
        peak = functools.reduce(jnp.maximum, pieces)
        total = sum(jnp.exp(piece - peak) for piece in pieces)
        factors[:, :width] = jnp.exp(peaks[:, :width] - (peak + jnp.log(total)))

    def join_terms(si):
        pieces, width = stat_pieces(si, 1, 0.0)
        row_terms[:, :width] = sum(pieces)

    def value_keys(si, p):
        columns = rows * (n - si)
        g32 = wide(qg_in, 1, p, n - si)
        g_all = g32.astype(bf16)
        v32 = own32(v_ref, half + p)
        total = None
        for h in range(2):
            row = 2 * p + h
            (g_own,) = own_lanes(h, g32)
            (v_own,) = own_lanes(h, v32)
            part_soft = raised[row, :, :columns] * factors[pl.ds(row, 1), :columns]
            raised[row, :, :columns] = part_soft
            total = plus(total, dot(part_soft.astype(bf16), g_own, PLAIN))
            soft_grad = dot(v_own, g_all, BY_LANES)
            value_dot[row, :, :columns] = soft_grad
            stats[1, si, pl.ds(row, 1), :columns] = jnp.sum(part_soft * soft_grad, axis=0, keepdims=True)
        vg[half + p] = total.astype(bf16)
        send_vg(half + p)

    def gradient_keys(si, p):
        columns = rows * (n - si)
        q32 = wide(qg_in, 0, p, n - si)
        k32 = own32(k_ref, half + p)
        dq = dk = None
        for h in range(2):
            row = 2 * p + h
            (q_own,) = own_lanes(h, q32)
            (k_own,) = own_lanes(h, k32)
            term = row_terms[pl.ds(row, 1), :columns]
            score_low = (raised[row, :, :columns] * (value_dot[row, :, :columns] - term)).astype(bf16)
            dk = plus(dk, dot(score_low, q_own, PLAIN))
            dq = plus(dq, dot(score_low, k_own, BY_ROWS))
        kg_ref[:, lanes(half + p)] = (dk * scale).astype(bf16)
        return dq * scale

    def pass_down(si, c, p, total):
        for b in range(si + 1):
            value = total[rows * b : rows * (b + 1)]
            if si < last:
                down_sum(c, b, p).wait_recv()
                value = value + down_in[c, p, b].astype(f32)
            value = value.astype(bf16)
            if b < si:
                down_out[c, p, b] = value
                down_sum(c, b, p).start()
            elif c == 0:
                vg[p] = value
                send_vg(p)
            else:
                kg_ref[:, lanes(p)] = value

    def pass_up(si, p, total):
        for j in range(n - si):
            value = total[rows * j : rows * (j + 1)]
            if si > 0:
                up_sum(j, p).wait_recv()
                value = value + up_in[p, j].astype(f32)
            value = value.astype(bf16)
            if j < last - si:
                up_out[p, j] = value
                up_sum(j, p).start()
            else:
                qg_ref[:, lanes(half + p)] = value

    def each(body):
        def step(p, carry):
            body(p)
            return carry

        lax.fori_loop(0, half, step, 0)

    def relay(si, a, t):
        if t == si + 1 and si < last and a == 0:
            for p in range(half):
                up(si, 1, si, p).start()
            hop(si, si, True).start()
        if t == n - si and si > 0 and a == 0:
            for p in range(half):
                down(si, 1, si, p).start()
            hop(si, si, False).start()
        for p in range(half):
            if si - t >= 0 and si < last:
                up_arrive(a, si - t, p)
                up(si, a, si - t, p).start()
            if si + t <= last and si > 0:
                down_arrive(a, si + t, p)
                down(si, a, si + t, p).start()

    def w_relay(si, t):
        if si - t >= 0:
            hop(si, si - t, True).wait_recv()
            if si < last:
                hop(si, si - t, True).start()
            w_start(si - t)
        if si + t <= last:
            hop(si, si + t, False).wait_recv()
            if si > 0:
                hop(si, si + t, False).start()
            w_start(si + t)

    def w_blocks(si, t):
        return [b for b in (si - t, si + t) if 0 <= b <= last]

    def first(si):
        columns, query_columns = rows * (si + 1), rows * (n - si)
        others = [u for u in range(n) if u != si]
        for p in range(half):
            if si < last:
                up(si, 0, si, p).start()
            if si > 0:
                down(si, 0, si, p).start()
        for u in others:
            gate_copy(si, u).start()
        w_start(si, True)
        for name in x_start:
            x_copy(name).start()

        for p in range(half):
            for a, ref in enumerate((k_ref, v_ref)):
                kv_in[a, p, si] = ref[:, lanes(p)]
            for a, ref in enumerate((q_ref, g_ref)):
                qg_in[a, p, last - si] = ref[:, lanes(half + p)]
        gate_pad[...] = jnp.zeros_like(gate_pad)
        for which in range(2):
            stats[which, si] = jnp.zeros(stats.shape[2:], f32)
        peaks[...] = jnp.zeros_like(peaks)
        held = gate_ref.shape[0]
        length = rows * n
        gate_pad[held * si : held * si + held, :length] = gate_ref[...]
        for u in others:
            gate_copy(u, u).wait_recv()
            gate_pad[held * u : held * u + held, :length] = gate_all[u]
        turned = gate_pad[...].T
        gate_t[...] = turned
        back = [turned[rows * b : rows * (b + 1)] for b in reversed(range(n))]
        gate_rev[...] = jnp.concatenate(back + [turned[length:]], axis=0).T

        for t in range(1, n):
            relay(si, 0, t)

        def queries_step(p):
            if si == last:
                for b in range(si):
                    up_arrive(0, b, p)
            total = softmax_queries(si, p)
            if si == last:
                pass_down(si, 0, p, total)
            else:
                down_acc[0, p, : si + 1] = total.reshape(si + 1, rows, LANES)

        def keys_step(p):
            if si == 0:
                for b in range(1, n):
                    down_arrive(0, b, p)
            softmax_keys(si, p)

        def do_keys():
            each(keys_step)
            for u in others:
                stat_copy(0, si, u).start()

        if 2 * si < n:
            each(queries_step)
            do_keys()
        else:
            do_keys()
            each(queries_step)
        x_all[d] = in_ref[...]
        w_all[d, si] = w_ref[...]
        x_middle()
        for t in range(1, n):
            relay(si, 1, t)
        w_middle(si)

        def value_step(p):
            if si == 0:
                for b in range(1, n):
                    down_arrive(1, b, p)
            value_keys(si, p)

        def do_values():
            for u in others:
                stat_copy(0, u, si).wait_recv()
            join_peaks(si)
            each(value_step)
            for u in others:
                stat_copy(1, si, u).start()

        def value_sums():
            if si < last:
                each(lambda p: pass_down(si, 0, p, down_acc[0, p, : si + 1].reshape(columns, LANES)))

        if 2 * si < n:
            do_values()
            value_sums()
        else:
            value_sums()
            do_values()
        w_last(si)
        w_relay(si, 1)
        x_last()

        def gradient_step(p):
            if si == last:
                for b in range(si):
                    up_arrive(1, b, p)
            total = gradient_queries(si, p)
            if si == last:
                pass_down(si, 1, p, total)
            else:
                down_acc[1, p, : si + 1] = total.reshape(si + 1, rows, LANES)

        each(gradient_step)
        w_relay(si, 2)
        for u in others:
            stat_copy(1, u, si).wait_recv()
        join_terms(si)

        def key_gradient_step(p):
            total = gradient_keys(si, p)
            if si == 0:
                pass_up(si, p, total)
            else:
                up_acc[p, : n - si] = total.reshape(n - si, rows, LANES)

        each(key_gradient_step)
        for j in w_blocks(si, 1):
            w_middle(j)

    def second(si, begin, end):
        for p in range(begin, end):
            if si < last:
                pass_down(si, 1, p, down_acc[1, p, : si + 1].reshape(rows * (si + 1), LANES))
            if si > 0:
                pass_up(si, p, up_acc[p, : n - si].reshape(rows * (n - si), LANES))

    def third(si):
        w_relay(si, 3)
        for j in w_blocks(si, 2):
            w_middle(j)
        for j in w_blocks(si, 1):
            w_last(j)
        for j in w_blocks(si, 3):
            w_middle(j)
        for t in (2, 3):
            for j in w_blocks(si, t):
                w_last(j)

    def finish(si):
        for p in range(half):
            for a in range(2):
                for b in range(si + 1):
                    if si < last:
                        up(si, a, b, p).wait_send()
                for b in range(si, n):
                    if si > 0:
                        down(si, a, b, p).wait_send()
            for c in range(2):
                for b in range(si):
                    down_sum(c, b, p).wait_send()
            for j in range(last - si):
                up_sum(j, p).wait_send()
        for u in range(n):
            if u != si:
                gate_copy(si, u).wait_send()
                for which in range(2):
                    stat_copy(which, si, u).wait_send()
        for b in range(n):
            if b <= si and si < last:
                hop(si, b, True).wait_send()
            if b >= si and si > 0:
                hop(si, b, False).wait_send()

    def by_device(body):
        for si in range(n):
            pl.when(s == si)(functools.partial(body, si))

    barrier = pltpu.get_barrier_semaphore()
    for r in range(1, n):
        pl.semaphore_signal(barrier, inc=1, device_id={"sp": (s + r) % n, "dp": d}, device_id_type=MESH)
    for step in range(1, 8):
        pl.semaphore_signal(barrier, inc=1, device_id={"sp": s, "dp": near(step)}, device_id_type=MESH)
    pl.semaphore_wait(barrier, n - 1 + 7)
    for copy in fetched:
        copy.wait()

    by_device(first)

    for name in ("own", "x over", "y over", "corner over"):
        x_copy(name).wait_recv()
    for i in range(2 * half):
        @pl.when(d != i)
        def _():
            k = sem("vg", 2 * half) + i
            remote(vg_seq.at[i], vg_seq.at[i], k, k, s, partner).wait_recv()

    def weight_part(j):
        columns = pl.ds(pl.multiple_of(j * block, LANES), block)
        total = None
        for i in range(8):
            total = plus(total, dot(vg_seq[i], x_all[i, :, columns], BY_ROWS))
        return total

    def part_copy(j, slot, to):
        return named(("part", slot), part.at[j], part_in.at[slot], to, d)

    mate, across = s + 1 - 2 * (s % 2), (s + 2) % n
    far = (mate + 2) % n
    part[far] = weight_part(far).astype(bf16)
    part_copy(far, 0, mate).start()
    part[mate] = weight_part(mate).astype(bf16)
    part_copy(mate, 1, mate).start()
    sum_ref[0] = weight_part(across)
    sum_ref[1] = weight_part(s)
    by_device(lambda si: second(si, 0, half // 2))
    part_copy(far, 0, mate).wait_recv()
    part[across] = (sum_ref[0] + part_in[0].astype(f32)).astype(bf16)
    part_copy(across, 2, across).start()
    by_device(lambda si: second(si, half // 2, half))
    by_device(third)

    for j in range(n):
        for name in ("own", "x over", "y over", "corner over"):
            w_copy(name, j).wait_recv()
    vg_rows = jnp.concatenate([vg[i] for i in range(8)], axis=1)
    for j in range(n):
        w_rows = jnp.concatenate([w_all[i, j] for i in range(8)], axis=1)
        ig_ref[:, j * block : (j + 1) * block] = dot(vg_rows, w_rows, BY_LANES).astype(bf16)

    by_device(finish)
    for name in x_start + x_rest:
        x_copy(name).wait_send()
    for j in range(n):
        for name in w_names:
            w_copy(name, j).wait_send()
    for p in range(2 * half):
        @pl.when(d != p)
        def _():
            vg_copy(p).wait_send()

    part_copy(mate, 1, mate).wait_recv()
    part_copy(across, 2, across).wait_recv()
    total = sum_ref[1] + part_in[1].astype(f32) + part_in[2].astype(f32)
    wg_ref[...] = total.T
    part_copy(far, 0, mate).wait_send()
    part_copy(mate, 1, mate).wait_send()
    part_copy(across, 2, across).wait_send()


def put_out(*refs):
    sems = refs[-1]
    copies = [pltpu.make_async_copy(refs[i], refs[4 + i], sems.at[i]) for i in range(4)]
    for copy in copies:
        copy.start()
    for copy in copies:
        copy.wait()


def fused(mesh, inputs, query, key, value, cotangent, gate, weight):
    n = mesh.shape["sp"]
    rows, width = query.shape[1:]
    model = inputs.shape[2]
    half = width // LANES // 2
    length = n * rows
    wide = padded(length)
    bf16, f32 = jnp.bfloat16, jnp.float32
    copies = 256
    vmem = pl.BlockSpec(memory_space=pltpu.VMEM)
    hbm = pl.BlockSpec(memory_space=pl.ANY)
    results = (
        jax.ShapeDtypeStruct((rows, width), bf16),
        jax.ShapeDtypeStruct((rows, width), bf16),
        jax.ShapeDtypeStruct((rows, model), bf16),
        jax.ShapeDtypeStruct((model // n, LANES), f32),
    )
    outs = pl.pallas_call(
        functools.partial(kernel, n, half),
        out_shape=tuple(pltpu.VMEM(x.shape, x.dtype) for x in results),
        in_specs=[hbm] * 5 + [vmem, hbm],
        out_specs=(vmem,) * 4,
        scratch_shapes=[
            pltpu.VMEM((rows, model), bf16),
            *[pltpu.VMEM((rows, width), bf16)] * 4,
            pltpu.VMEM((model // n, LANES), bf16),
            *[pltpu.VMEM((2, half, n, rows, LANES), bf16)] * 2,
            *[pltpu.VMEM((2, half, n - 1, rows, LANES), bf16)] * 2,
            *[pltpu.VMEM((half, n - 1, rows, LANES), bf16)] * 2,
            pltpu.VMEM((2, half, n, rows, LANES), f32),
            pltpu.VMEM((half, n, rows, LANES), f32),
            pltpu.VMEM((8, rows, LANES), bf16),
            pltpu.VMEM((8, rows, LANES), bf16),
            pltpu.VMEM((8, rows, model), bf16),
            pltpu.VMEM((8, n, model // n, LANES), bf16),
            pltpu.VMEM((n, LANES, model // n), bf16),
            pltpu.VMEM((3, LANES, model // n), bf16),
            pltpu.VMEM((2, LANES, model // n), f32),
            pltpu.VMEM((n, gate.shape[1], length), f32),
            pltpu.VMEM((LANES, wide), f32),
            pltpu.VMEM((wide, LANES), f32),
            pltpu.VMEM((LANES, wide), f32),
            *[pltpu.VMEM((2 * half, rows, length), f32)] * 3,
            *[pltpu.VMEM((2 * half, wide), f32)] * 3,
            pltpu.VMEM((2, n, 2 * half, wide), f32),
            pltpu.SemaphoreType.DMA((6,)),
            pltpu.SemaphoreType.DMA((copies,)),
            pltpu.SemaphoreType.DMA((copies,)),
        ],
        compiler_params=pltpu.CompilerParams(
            collective_id=0, has_side_effects=True, vmem_limit_bytes=60 * 2**20
        ),
    )(inputs[0], query[0], key[0], value[0], cotangent[0], gate[0], weight)
    query_grad, key_grad, input_grad, weight_grad = pl.pallas_call(
        put_out,
        out_shape=results,
        in_specs=[vmem] * 4,
        out_specs=(hbm,) * 4,
        scratch_shapes=[pltpu.SemaphoreType.DMA((4,))],
        compiler_params=pltpu.CompilerParams(vmem_limit_bytes=2**20),
    )(*(pltpu.with_memory_space_constraint(x, pltpu.VMEM) for x in outs))
    return (query_grad[None], key_grad[None], input_grad[None], weight_grad)


def solution(mesh):
    in_specs = (
        P("dp", "sp", None),
        P("dp", "sp", None),
        P("dp", "sp", None),
        P("dp", "sp", None),
        P("dp", "sp", None),
        P("dp", "sp", None),
        P("sp", "dp"),
    )
    out_specs = (P("dp", "sp", None), P("dp", "sp", None), P("dp", "sp", None), P("sp", "dp"))
    sp_count, dp_count = mesh.shape["sp"], mesh.shape["dp"]

    def per_device(*arrays):
        if one_kernel_fits(sp_count, dp_count, *arrays):
            return fused(mesh, *arrays)
        return shards(*arrays)

    return jax.shard_map(per_device, mesh=mesh, in_specs=in_specs, out_specs=out_specs, check_vma=False)
```

time: 65.1 us -> 89.1 us (1.37)
  Pallas kernels: 63.7 us -> 87.1 us
    pallas_call x1, Pallas kernels: 62.6 us -> 86 us  [fused(): pl.pallas_call(functools.partial(kernel, n, half), out_shape=tuple((pltpu...]
where the time goes in v1:
time: 89.1 us; the launch traced here: 87.9 us
  Pallas kernels  87.1 us (98%)
    pallas_call x1, Pallas kernels, fused(): pl.pallas_call(functools.partial(kernel, n, half), out_shape=tuple((pltpu...  86 us

profile of v1, /device:TPU:1, one launch (start us, length us, event | category | flops | bytes accessed | tf_op | source)
XLA Modules:
  0.0 87.9 jit_solution(10631729695990883071)
XLA Ops:
  0.6 86.0 %shard_map.102 = (bf16[136,1024]{1,0:T(8,128)(2,1)S(1)}, bf16[136,1024]{1,0:T(8,128)(2,1)S(1)}, bf16[136,2048]{1,0:T(8,128)(2,1)S(1)}, f32[512,128]{1,0:T(8,128)S(1)}) custom-call(bf16[136,2048]{1,0:T(8,128)(2,1)} %bitcast.9, bf16[136,1024]{1,0:T(8,128)(2,1)} %bitcast.10, bf16[136,1024]{1,0:T(8,128)(2,1)} %bitcast.11, bf16[136,1024]{1,0:T(8,128)(2,1)} %bitcast.12, ...), custom_call_target="tpu_custom_call" | custom-call | tf_op jit(solution)/shard_map/pallas_call | solution.py:814
  86.7 1.1 %shard_map.103 = (bf16[136,1024]{1,0:T(8,128)(2,1)}, bf16[136,1024]{1,0:T(8,128)(2,1)}, bf16[136,2048]{1,0:T(8,128)(2,1)}, f32[512,128]{1,0:T(8,128)}) custom-call(bf16[136,1024]{1,0:T(8,128)(2,1)S(1)} %get-tuple-element.12.refs_0_, bf16[136,1024]{1,0:T(8,128)(2,1)S(1)} %get-tuple-element.13.refs_1_, bf16[136,2048]{1,0:T(8,128)(2,1)S(1)} %get-tuple-element.14.refs_2_, ...), custom_call_target="tpu_custom_call" | custom-call | tf_op jit(solution)/shard_map/pallas_call | solution.py:850

commit v2 on v1

--- a/solution.py
+++ b/solution.py
@@ -206,10 +206,14 @@
         if key not in ids:
             ids[key] = used[0]
             used[0] += count
-            assert used[0] <= send_sems.shape[0]
+            assert used[0] <= recv_sems.shape[0], (key, used, recv_sems.shape)
         return ids[key]
 
-    def remote(src, dst, send_id, recv_id, to_sp, to_dp):
+    sent_ids = {}
+
+    def remote(src, dst, kind, recv_id, to_sp, to_dp):
+        send_id = sent_ids.setdefault(kind, len(sent_ids))
+        assert send_id < send_sems.shape[0]
         return pltpu.make_async_remote_copy(
             src_ref=src,
             dst_ref=dst,
@@ -219,39 +223,40 @@
             device_id_type=MESH,
         )
 
-    def named(name, src, dst, to_sp, to_dp):
-        i = sem(name)
-        return remote(src, dst, i, i, to_sp, to_dp)
+    def sent(kind, ref):
+        remote(ref, ref, kind, 0, s, partner).wait_send()
+
+    def arrived(name, ref):
+        remote(ref, ref, "up", sem(name), s, partner).wait_recv()
 
     def up(si, a, b, p):
         src = (k_ref, v_ref)[a].at[:, lanes(p)] if b == si else kv_in.at[a, p, b]
         i = sem(("up", a, b), half) + p
-        return remote(src, kv_in.at[a, p, b], i, i, s + 1, d)
+        return remote(src, kv_in.at[a, p, b], "up", i, s + 1, d)
 
     def up_arrive(a, b, p):
         i = sem(("up", a, b), half) + p
-        remote(kv_in.at[a, p, b], kv_in.at[a, p, b], i, i, (s + 1) % n, d).wait_recv()
+        remote(kv_in.at[a, p, b], kv_in.at[a, p, b], "up", i, (s + 1) % n, d).wait_recv()
 
     def down(si, a, b, p):
         src = (q_ref, g_ref)[a].at[:, lanes(half + p)] if b == si else qg_in.at[a, p, last - b]
         i = sem(("down", a, b), half) + p
-        return remote(src, qg_in.at[a, p, last - b], i, i, s - 1, d)
+        return remote(src, qg_in.at[a, p, last - b], "down", i, s - 1, d)
 
     def down_arrive(a, b, p):
         i = sem(("down", a, b), half) + p
-        remote(qg_in.at[a, p, last - b], qg_in.at[a, p, last - b], i, i, (s + 1) % n, d).wait_recv()
+        remote(qg_in.at[a, p, last - b], qg_in.at[a, p, last - b], "down", i, (s + 1) % n, d).wait_recv()
 
     def down_sum(c, b, p):
         i = sem(("down sum", c, b), half) + p
-        return remote(down_out.at[c, p, b], down_in.at[c, p, b], i, i, (s + n - 1) % n, d)
+        return remote(down_out.at[c, p, b], down_in.at[c, p, b], "down sum", i, (s + n - 1) % n, d)
 
     def up_sum(j, p):
         i = sem(("up sum", j), half) + p
-        return remote(up_out.at[p, j], up_in.at[p, j], i, i, (s + 1) % n, d)
+        return remote(up_out.at[p, j], up_in.at[p, j], "up sum", i, (s + 1) % n, d)
 
     def gate_copy(sender, to):
-        i = sem("gate", n)
-        return remote(gate_ref, gate_all.at[sender], i + to, i + sender, to, d)
+        return remote(gate_ref, gate_all.at[sender], "gate", sem("gate"), to, d)
 
     def stat_width(a, b):
         return padded(rows * (n - max(a, b)))
@@ -259,16 +264,15 @@
     def stat_copy(which, sender, to):
         i = sem(("stat", which), n)
         piece = stats.at[which, sender, :, pl.ds(0, stat_width(sender, to))]
-        return remote(piece, piece, i + to, i + sender, to, d)
+        return remote(piece, piece, ("stat", which), i + sender, to, d)
 
     def hop(si, b, upward):
         src = w_ref if b == si else w_all.at[d, b]
         i = sem(("hop", upward), n) + b
-        return remote(src, w_all.at[d, b], i, i, (s + 1) % n if upward else (s + n - 1) % n, d)
+        return remote(src, w_all.at[d, b], ("hop", upward), i, (s + 1) % n if upward else (s + n - 1) % n, d)
 
     def vg_copy(p):
-        i = sem("vg", 2 * half)
-        return remote(vg.at[p], vg_seq.at[d], i + p, i + d, s, p)
+        return remote(vg.at[p], vg_seq.at[d], "vg", sem("vg"), s, p)
 
     def send_vg(p):
         @pl.when(d != p)
@@ -280,54 +284,55 @@
             vg_seq[p] = vg[p]
 
     def x_copy(name):
-        return {
-            "x low": lambda: named(name, in_ref.at[:, low], x_all.at[d, :, low], s, x_near),
-            "x high": lambda: named(name, in_ref.at[:, high], x_all.at[d, :, high], s, x_near),
-            "y high": lambda: named(name, in_ref.at[:, high], x_all.at[d, :, high], s, y_near),
-            "y low": lambda: named(name, in_ref.at[:, low], x_all.at[d, :, low], s, y_near),
-            "own": lambda: named(name, in_ref, x_all.at[d], s, partner),
-            "on y": lambda: named(name, x_all.at[x_near, :, low], x_all.at[x_near, :, low], s, y_near),
-            "on x": lambda: named(name, x_all.at[y_near, :, high], x_all.at[y_near, :, high], s, x_near),
-            "x over": lambda: named(name, x_all.at[x_near], x_all.at[x_near], s, partner),
-            "y over": lambda: named(name, x_all.at[y_near], x_all.at[y_near], s, partner),
-            "corner over": lambda: named(name, x_all.at[corner], x_all.at[corner], s, partner),
-        }[name]()
+        src, dst, to = {
+            "x low": (in_ref.at[:, low], x_all.at[d, :, low], x_near),
+            "x high": (in_ref.at[:, high], x_all.at[d, :, high], x_near),
+            "y high": (in_ref.at[:, high], x_all.at[d, :, high], y_near),
+            "y low": (in_ref.at[:, low], x_all.at[d, :, low], y_near),
+            "own": (in_ref, x_all.at[d], partner),
+            "on y": (x_all.at[x_near, :, low],) * 2 + (y_near,),
+            "on x": (x_all.at[y_near, :, high],) * 2 + (x_near,),
+            "x over": (x_all.at[x_near],) * 2 + (partner,),
+            "y over": (x_all.at[y_near],) * 2 + (partner,),
+            "corner over": (x_all.at[corner],) * 2 + (partner,),
+        }[name]
+        key = "x on" if name[:2] == "on" else "x over" if name[-4:] == "over" or name == "own" else name
+        return remote(src, dst, "x", sem(("x", key)), s, to)
 
     x_start = ("x low", "y high", "x high", "y low", "own")
-    x_rest = ("on y", "on x", "x over", "y over", "corner over")
 
     def x_middle():
         x_copy("x low").wait_recv()
         x_copy("on y").start()
         x_copy("y high").wait_recv()
         x_copy("on x").start()
+
+    def x_over():
         x_copy("x high").wait_recv()
         x_copy("x over").start()
         x_copy("y low").wait_recv()
         x_copy("y over").start()
 
     def x_last():
-        x_copy("on y").wait_recv()
-        x_copy("on x").wait_recv()
+        arrived(("x", "x on"), x_all.at[corner])
         x_copy("corner over").start()
 
     w_lower, w_upper = pl.ds(0, block // 2), pl.ds(block // 2, block // 2)
 
     def w_copy(name, j, own=False):
-        src = w_ref if own else w_all.at[d, j]
-        key = ("w", name, j)
-        return {
-            "x": lambda: named(key, src, w_all.at[d, j], s, x_near),
-            "y": lambda: named(key, src, w_all.at[d, j], s, y_near),
-            "own": lambda: named(key, src, w_all.at[d, j], s, partner),
-            "on y": lambda: named(key, w_all.at[x_near, j, w_lower], w_all.at[x_near, j, w_lower], s, y_near),
-            "on x": lambda: named(key, w_all.at[y_near, j, w_upper], w_all.at[y_near, j, w_upper], s, x_near),
-            "x over": lambda: named(key, w_all.at[x_near, j], w_all.at[x_near, j], s, partner),
-            "y over": lambda: named(key, w_all.at[y_near, j], w_all.at[y_near, j], s, partner),
-            "corner over": lambda: named(key, w_all.at[corner, j], w_all.at[corner, j], s, partner),
-        }[name]()
-
-    w_names = ("x", "y", "own", "on y", "on x", "x over", "y over", "corner over")
+        first = w_ref if own else w_all.at[d, j]
+        src, dst, to = {
+            "x": (first, w_all.at[d, j], x_near),
+            "y": (first, w_all.at[d, j], y_near),
+            "own": (first, w_all.at[d, j], partner),
+            "on y": (w_all.at[x_near, j, w_lower],) * 2 + (y_near,),
+            "on x": (w_all.at[y_near, j, w_upper],) * 2 + (x_near,),
+            "x over": (w_all.at[x_near, j],) * 2 + (partner,),
+            "y over": (w_all.at[y_near, j],) * 2 + (partner,),
+            "corner over": (w_all.at[corner, j],) * 2 + (partner,),
+        }[name]
+        key = ("on", j) if name[:2] == "on" else "over" if name[-4:] == "over" or name == "own" else (name, j)
+        return remote(src, dst, "w", sem(("w", key)), s, to)
 
     def w_start(j, own=False):
         for name in ("x", "y", "own"):
@@ -342,8 +347,7 @@
         w_copy("y over", j).start()
 
     def w_last(j):
-        w_copy("on y", j).wait_recv()
-        w_copy("on x", j).wait_recv()
+        arrived(("w", ("on", j)), w_all.at[corner, j])
         w_copy("corner over", j).start()
 
     def wide(buffer, a, p, count):
@@ -500,41 +504,59 @@
             else:
                 qg_ref[:, lanes(half + p)] = value
 
-    def each(body):
+    def each(body, begin=0, end=half):
         def step(p, carry):
             body(p)
             return carry
 
-        lax.fori_loop(0, half, step, 0)
+        lax.fori_loop(begin, end, step, 0)
+
+    def relay_up(si, a, t, p):
+        if si - t >= 0 and si < last:
+            up_arrive(a, si - t, p)
+            up(si, a, si - t, p).start()
+
+    def relay_down(si, a, t, p):
+        if si + t <= last and si > 0:
+            down_arrive(a, si + t, p)
+            down(si, a, si + t, p).start()
+
+    def send_own(si, upward, begin, end):
+        for p in range(begin, end):
+            (up if upward else down)(si, 1, si, p).start()
 
     def relay(si, a, t):
-        if t == si + 1 and si < last and a == 0:
-            for p in range(half):
-                up(si, 1, si, p).start()
-            hop(si, si, True).start()
-        if t == n - si and si > 0 and a == 0:
-            for p in range(half):
-                down(si, 1, si, p).start()
-            hop(si, si, False).start()
         for p in range(half):
-            if si - t >= 0 and si < last:
-                up_arrive(a, si - t, p)
-                up(si, a, si - t, p).start()
-            if si + t <= last and si > 0:
-                down_arrive(a, si + t, p)
-                down(si, a, si + t, p).start()
-
-    def w_relay(si, t):
+            relay_up(si, a, t, p)
+            relay_down(si, a, t, p)
+
+    def relay_first(si):
+        if si in (0, last):
+            return
+        upper = 2 * si >= n
+        relay(si, 0, 1)
+        send_own(si, not upper, 0, half)
+        for t in range(2, n):
+            relay(si, 0, t)
+        send_own(si, upper, 0, half)
+
+    def w_relay_up(si, t):
         if si - t >= 0:
             hop(si, si - t, True).wait_recv()
             if si < last:
                 hop(si, si - t, True).start()
             w_start(si - t)
+
+    def w_relay_down(si, t):
         if si + t <= last:
             hop(si, si + t, False).wait_recv()
             if si > 0:
                 hop(si, si + t, False).start()
             w_start(si + t)
+
+    def w_relay(si, t):
+        w_relay_up(si, t)
+        w_relay_down(si, t)
 
     def w_blocks(si, t):
         return [b for b in (si - t, si + t) if 0 <= b <= last]
@@ -549,15 +571,23 @@
                 down(si, 0, si, p).start()
         for u in others:
             gate_copy(si, u).start()
-        w_start(si, True)
+        if si == 0:
+            send_own(si, True, 0, half)
+            hop(si, si, True).start()
+        if si == last:
+            send_own(si, False, 0, half)
+            hop(si, si, False).start()
         for name in x_start:
             x_copy(name).start()
+        w_start(si, True)
 
         for p in range(half):
             for a, ref in enumerate((k_ref, v_ref)):
                 kv_in[a, p, si] = ref[:, lanes(p)]
             for a, ref in enumerate((q_ref, g_ref)):
                 qg_in[a, p, last - si] = ref[:, lanes(half + p)]
+        relay_first(si)
+
         gate_pad[...] = jnp.zeros_like(gate_pad)
         for which in range(2):
             stats[which, si] = jnp.zeros(stats.shape[2:], f32)
@@ -565,18 +595,16 @@
         held = gate_ref.shape[0]
         length = rows * n
         gate_pad[held * si : held * si + held, :length] = gate_ref[...]
+        arrived("gate", gate_all.at[:last])
         for u in others:
-            gate_copy(u, u).wait_recv()
             gate_pad[held * u : held * u + held, :length] = gate_all[u]
         turned = gate_pad[...].T
         gate_t[...] = turned
         back = [turned[rows * b : rows * (b + 1)] for b in reversed(range(n))]
         gate_rev[...] = jnp.concatenate(back + [turned[length:]], axis=0).T
 
-        for t in range(1, n):
-            relay(si, 0, t)
-
         def queries_step(p):
+            relay_up(si, 1, 1, p)
             if si == last:
                 for b in range(si):
                     up_arrive(0, b, p)
@@ -587,56 +615,11 @@
                 down_acc[0, p, : si + 1] = total.reshape(si + 1, rows, LANES)
 
         def keys_step(p):
+            relay_down(si, 1, 1, p)
             if si == 0:
                 for b in range(1, n):
                     down_arrive(0, b, p)
             softmax_keys(si, p)
-
-        def do_keys():
-            each(keys_step)
-            for u in others:
-                stat_copy(0, si, u).start()
-
-        if 2 * si < n:
-            each(queries_step)
-            do_keys()
-        else:
-            do_keys()
-            each(queries_step)
-        x_all[d] = in_ref[...]
-        w_all[d, si] = w_ref[...]
-        x_middle()
-        for t in range(1, n):
-            relay(si, 1, t)
-        w_middle(si)
-
-        def value_step(p):
-            if si == 0:
-                for b in range(1, n):
-                    down_arrive(1, b, p)
-            value_keys(si, p)
-
-        def do_values():
-            for u in others:
-                stat_copy(0, u, si).wait_recv()
-            join_peaks(si)
-            each(value_step)
-            for u in others:
-                stat_copy(1, si, u).start()
-
-        def value_sums():
-            if si < last:
-                each(lambda p: pass_down(si, 0, p, down_acc[0, p, : si + 1].reshape(columns, LANES)))
-
-        if 2 * si < n:
-            do_values()
-            value_sums()
-        else:
-            value_sums()
-            do_values()
-        w_last(si)
-        w_relay(si, 1)
-        x_last()
 
         def gradient_step(p):
             if si == last:
@@ -648,11 +631,50 @@
             else:
                 down_acc[1, p, : si + 1] = total.reshape(si + 1, rows, LANES)
 
-        each(gradient_step)
-        w_relay(si, 2)
-        for u in others:
-            stat_copy(1, u, si).wait_recv()
-        join_terms(si)
+        def do_keys():
+            each(keys_step)
+            for u in others:
+                stat_copy(0, si, u).start()
+
+        if si == 0:
+            each(queries_step)
+            each(gradient_step)
+            do_keys()
+        elif 2 * si < n:
+            each(queries_step)
+            hop(si, si, True).start()
+            do_keys()
+        else:
+            do_keys()
+            each(queries_step)
+        x_middle()
+        for t in range(2, n):
+            relay(si, 1, t)
+        if 0 < si < last:
+            if 2 * si < n:
+                hop(si, si, False).start()
+                w_relay_up(si, 1)
+            else:
+                hop(si, si, True).start()
+        x_all[d] = in_ref[...]
+        w_all[d, si] = w_ref[...]
+
+        def value_step(p):
+            if si == 0:
+                for b in range(1, n):
+                    down_arrive(1, b, p)
+            value_keys(si, p)
+
+        def do_values():
+            for u in others:
+                stat_copy(0, u, si).wait_recv()
+            join_peaks(si)
+            each(value_step)
+            for u in others:
+                stat_copy(1, si, u).start()
+
+        def value_sums(begin=0, end=half):
+            each(lambda p: pass_down(si, 0, p, down_acc[0, p, : si + 1].reshape(columns, LANES)), begin, end)
 
         def key_gradient_step(p):
             total = gradient_keys(si, p)
@@ -661,53 +683,102 @@
             else:
                 up_acc[p, : n - si] = total.reshape(n - si, rows, LANES)
 
-        each(key_gradient_step)
+        def do_key_gradients():
+            for u in others:
+                stat_copy(1, u, si).wait_recv()
+            join_terms(si)
+            each(key_gradient_step)
+
+        if si == 0:
+            do_values()
+            x_over()
+            do_key_gradients()
+            value_sums()
+            x_last()
+            w_middle(si)
+            w_relay(si, 1)
+        elif si == last:
+            do_values()
+            x_over()
+            w_middle(si)
+            each(gradient_step)
+            x_last()
+            w_relay(si, 1)
+            do_key_gradients()
+            w_relay(si, 2)
+        elif 2 * si < n:
+            do_values()
+            x_over()
+            w_middle(si)
+            value_sums()
+            w_relay_down(si, 1)
+            each(gradient_step)
+            x_last()
+            do_key_gradients()
+            w_relay(si, 2)
+        else:
+            value_sums(0, half // 2)
+            do_values()
+            value_sums(half // 2, half)
+            hop(si, si, False).start()
+            w_relay_down(si, 1)
+            x_over()
+            w_middle(si)
+            w_relay_up(si, 1)
+            each(gradient_step)
+            x_last()
+            w_relay(si, 2)
+            do_key_gradients()
+
+    def chain_down(si, begin, end):
+        if si < last:
+            for p in range(begin, end):
+                pass_down(si, 1, p, down_acc[1, p, : si + 1].reshape(rows * (si + 1), LANES))
+
+    def chain_up(si, begin, end):
+        if si > 0:
+            for p in range(begin, end):
+                pass_up(si, p, up_acc[p, : n - si].reshape(rows * (n - si), LANES))
+
+    def chain_first(si, begin, end):
+        (chain_up if 2 * si < n else chain_down)(si, begin, end)
+
+    def chain_rest(si):
+        (chain_down if 2 * si < n else chain_up)(si, 0, half)
+
+    def fourth(si):
+        if si == 0:
+            w_relay(si, 2)
+        w_relay(si, 3)
         for j in w_blocks(si, 1):
             w_middle(j)
 
-    def second(si, begin, end):
-        for p in range(begin, end):
-            if si < last:
-                pass_down(si, 1, p, down_acc[1, p, : si + 1].reshape(rows * (si + 1), LANES))
-            if si > 0:
-                pass_up(si, p, up_acc[p, : n - si].reshape(rows * (n - si), LANES))
-
     def third(si):
-        w_relay(si, 3)
         for j in w_blocks(si, 2):
             w_middle(j)
+        for j in w_blocks(si, 3):
+            w_middle(j)
+        chain_rest(si)
+        w_last(si)
         for j in w_blocks(si, 1):
             w_last(j)
-        for j in w_blocks(si, 3):
-            w_middle(j)
         for t in (2, 3):
             for j in w_blocks(si, t):
                 w_last(j)
 
     def finish(si):
-        for p in range(half):
-            for a in range(2):
-                for b in range(si + 1):
-                    if si < last:
-                        up(si, a, b, p).wait_send()
-                for b in range(si, n):
-                    if si > 0:
-                        down(si, a, b, p).wait_send()
-            for c in range(2):
-                for b in range(si):
-                    down_sum(c, b, p).wait_send()
-            for j in range(last - si):
-                up_sum(j, p).wait_send()
-        for u in range(n):
-            if u != si:
-                gate_copy(si, u).wait_send()
-                for which in range(2):
-                    stat_copy(which, si, u).wait_send()
-        for b in range(n):
-            if b <= si and si < last:
-                hop(si, b, True).wait_send()
-            if b >= si and si > 0:
-                hop(si, b, False).wait_send()
+        if si < last:
+            sent("up", kv_in.at[:, :, : si + 1])
+            sent("up sum", up_out.at[:, : last - si])
+            sent(("hop", True), w_all.at[0, : si + 1])
+        if si > 0:
+            sent("down", qg_in.at[:, :, : n - si])
+            sent("down sum", down_out.at[:, :, :si])
+            sent(("hop", False), w_all.at[0, : n - si])
+        width = sum(stat_width(si, u) for u in range(n) if u != si)
+        count = next(c for c in range(1, n + 1) if width % (c * LANES) == 0 and width // c <= stats.shape[3])
+        for which in range(2):
+            sent(("stat", which), stats.at[0, :count, :, : width // count])
 
     def by_device(body):
         for si in range(n):
@@ -724,13 +795,8 @@
 
     by_device(first)
 
-    for name in ("own", "x over", "y over", "corner over"):
-        x_copy(name).wait_recv()
-    for i in range(2 * half):
-        @pl.when(d != i)
-        def _():
-            k = sem("vg", 2 * half) + i
-            remote(vg_seq.at[i], vg_seq.at[i], k, k, s, partner).wait_recv()
+    arrived(("x", "x over"), x_all.at[:4])
+    arrived("vg", vg_seq.at[:7])
 
     def weight_part(j):
         columns = pl.ds(pl.multiple_of(j * block, LANES), block)
@@ -739,50 +805,56 @@
             total = plus(total, dot(vg_seq[i], x_all[i, :, columns], BY_ROWS))
         return total
 
+    side = s // 2
+    mate = s + 1 - 2 * (s % 2)
+    outer = (s == 0) | (s == last)
+    inner = (s > 0) & (s < last)
+    outermost, nearest = (1 - side) * last, 2 - side
+
     def part_copy(j, slot, to):
-        return named(("part", slot), part.at[j], part_in.at[slot], to, d)
-
-    mate, across = s + 1 - 2 * (s % 2), (s + 2) % n
-    far = (mate + 2) % n
-    part[far] = weight_part(far).astype(bf16)
-    part_copy(far, 0, mate).start()
-    part[mate] = weight_part(mate).astype(bf16)
-    part_copy(mate, 1, mate).start()
-    sum_ref[0] = weight_part(across)
-    sum_ref[1] = weight_part(s)
-    by_device(lambda si: second(si, 0, half // 2))
-    part_copy(far, 0, mate).wait_recv()
-    part[across] = (sum_ref[0] + part_in[0].astype(f32)).astype(bf16)
-    part_copy(across, 2, across).start()
-    by_device(lambda si: second(si, half // 2, half))
+        return remote(part.at[j], part_in.at[slot], "part", sem("part", 4) + slot, to, d)
+
+    def give(j, k, slot):
+        part[j] = sum_ref[k].astype(bf16)
+        part_copy(j, slot, mate).start()
+
+    sum_ref[0] = weight_part(jnp.where(outer, outermost, mate))
+    pl.when(outer)(lambda: give(outermost, 0, 0))
+    pl.when(inner)(lambda: give(mate, 0, 2))
+    sum_ref[1] = weight_part(jnp.where(outer, nearest, outermost))
+    pl.when(outer)(lambda: give(nearest, 1, 1))
+    sum_ref[2] = weight_part(jnp.where(outer, mate, nearest))
+    pl.when(outer)(lambda: give(mate, 2, 2))
+    sum_ref[3] = weight_part(s)
+    by_device(fourth)
+    by_device(lambda si: chain_first(si, 0, half))
+
+    @pl.when(inner)
+    def _():
+        for k, j in ((0, outermost), (1, nearest)):
+            part_copy(j, k, j).wait_recv()
+            part[j] = (sum_ref[k + 1] + part_in[k].astype(f32)).astype(bf16)
+            part_copy(j, 3, j).start()
+
     by_device(third)
 
-    for j in range(n):
-        for name in ("own", "x over", "y over", "corner over"):
-            w_copy(name, j).wait_recv()
+    arrived(("w", "over"), w_all.at[:4])
     vg_rows = jnp.concatenate([vg[i] for i in range(8)], axis=1)
     for j in range(n):
         w_rows = jnp.concatenate([w_all[i, j] for i in range(8)], axis=1)
         ig_ref[:, j * block : (j + 1) * block] = dot(vg_rows, w_rows, BY_LANES).astype(bf16)
 
     by_device(finish)
-    for name in x_start + x_rest:
-        x_copy(name).wait_send()
-    for j in range(n):
-        for name in w_names:
-            w_copy(name, j).wait_send()
-    for p in range(2 * half):
-        @pl.when(d != p)
-        def _():
-            vg_copy(p).wait_send()
-
-    part_copy(mate, 1, mate).wait_recv()
-    part_copy(across, 2, across).wait_recv()
-    total = sum_ref[1] + part_in[1].astype(f32) + part_in[2].astype(f32)
+    sent("gate", gate_all.at[:last])
+    sent("vg", vg_seq.at[:7])
+    sent("x", x_all.at[:7])
+    sent("w", w_all.at[:7])
+
+    for slot in (2, 3):
+        part_copy(s, slot, mate).wait_recv()
+    total = sum_ref[3] + part_in[2].astype(f32) + part_in[3].astype(f32)
     wg_ref[...] = total.T
-    part_copy(far, 0, mate).wait_send()
-    part_copy(mate, 1, mate).wait_send()
-    part_copy(across, 2, across).wait_send()
+    sent("part", part.at[:3])
 
 
 def put_out(*refs):
@@ -802,7 +874,7 @@
     length = n * rows
     wide = padded(length)
     bf16, f32 = jnp.bfloat16, jnp.float32
-    copies = 256
+    copies = 7 * (n - 1) * half + 7 * n + 13
     vmem = pl.BlockSpec(memory_space=pltpu.VMEM)
     hbm = pl.BlockSpec(memory_space=pl.ANY)
     results = (
@@ -830,8 +902,8 @@
             pltpu.VMEM((8, rows, model), bf16),
             pltpu.VMEM((8, n, model // n, LANES), bf16),
             pltpu.VMEM((n, LANES, model // n), bf16),
-            pltpu.VMEM((3, LANES, model // n), bf16),
-            pltpu.VMEM((2, LANES, model // n), f32),
+            pltpu.VMEM((4, LANES, model // n), bf16),
+            pltpu.VMEM((4, LANES, model // n), f32),
             pltpu.VMEM((n, gate.shape[1], length), f32),
             pltpu.VMEM((LANES, wide), f32),
             pltpu.VMEM((wide, LANES), f32),
@@ -840,7 +912,7 @@
             *[pltpu.VMEM((2 * half, wide), f32)] * 3,
             pltpu.VMEM((2, n, 2 * half, wide), f32),
             pltpu.SemaphoreType.DMA((6,)),
-            pltpu.SemaphoreType.DMA((copies,)),
+            pltpu.SemaphoreType.DMA((13,)),
             pltpu.SemaphoreType.DMA((copies,)),
         ],
         compiler_params=pltpu.CompilerParams(

time: 89.1 us -> 58.6 us (0.66); the launches traced: 87.9 us -> 58.4 us
  Pallas kernels: 87.1 us -> 57.8 us
    pallas_call x1, Pallas kernels: 86 us -> 56.6 us  [fused(): pl.pallas_call(functools.partial(kernel, n, half), out_shape=tuple((pltpu...]
where the time goes in v2:
time: 58.6 us; the launch traced here: 58.4 us
  Pallas kernels  57.8 us (99%)
  between operations  0.64 us (1%)
    pallas_call x1, Pallas kernels, fused(): pl.pallas_call(functools.partial(kernel, n, half), out_shape=tuple((pltpu...  56.6 us

profile of v2, /device:TPU:1, one launch (start us, length us, event | category | flops | bytes accessed | tf_op | source)
XLA Modules:
  0.0 58.4 jit_solution(1294292037732001816)
XLA Ops:
  0.6 56.6 %shard_map.102 = (bf16[136,1024]{1,0:T(8,128)(2,1)S(1)}, bf16[136,1024]{1,0:T(8,128)(2,1)S(1)}, bf16[136,2048]{1,0:T(8,128)(2,1)S(1)}, f32[512,128]{1,0:T(8,128)S(1)}) custom-call(bf16[136,2048]{1,0:T(8,128)(2,1)} %bitcast.9, bf16[136,1024]{1,0:T(8,128)(2,1)} %bitcast.10, bf16[136,1024]{1,0:T(8,128)(2,1)} %bitcast.11, bf16[136,1024]{1,0:T(8,128)(2,1)} %bitcast.12, ...), custom_call_target="tpu_custom_call" | custom-call | tf_op jit(solution)/shard_map/pallas_call | solution.py:886
  57.3 1.1 %shard_map.103 = (bf16[136,1024]{1,0:T(8,128)(2,1)}, bf16[136,1024]{1,0:T(8,128)(2,1)}, bf16[136,2048]{1,0:T(8,128)(2,1)}, f32[512,128]{1,0:T(8,128)}) custom-call(bf16[136,1024]{1,0:T(8,128)(2,1)S(1)} %get-tuple-element.12.refs_0_, bf16[136,1024]{1,0:T(8,128)(2,1)S(1)} %get-tuple-element.13.refs_1_, bf16[136,2048]{1,0:T(8,128)(2,1)S(1)} %get-tuple-element.14.refs_2_, ...), custom_call_target="tpu_custom_call" | custom-call | tf_op jit(solution)/shard_map/pallas_call | solution.py:922

commit v3 on v2

--- a/solution.py
+++ b/solution.py
@@ -331,7 +331,9 @@
             "y over": (w_all.at[y_near, j],) * 2 + (partner,),
             "corner over": (w_all.at[corner, j],) * 2 + (partner,),
         }[name]
-        key = ("on", j) if name[:2] == "on" else "over" if name[-4:] == "over" or name == "own" else (name, j)
+        if name[-4:] == "over" or name == "own":
+            return remote(src, dst, "w", sem("w over", n) + j, s, to)
+        key = ("on", j) if name[:2] == "on" else (name, j)
         return remote(src, dst, "w", sem(("w", key)), s, to)
 
     def w_start(j, own=False):
@@ -615,7 +617,8 @@
                 down_acc[0, p, : si + 1] = total.reshape(si + 1, rows, LANES)
 
         def keys_step(p):
-            relay_down(si, 1, 1, p)
+            if 2 * si >= n:
+                relay_down(si, 1, 1, p)
             if si == 0:
                 for b in range(1, n):
                     down_arrive(0, b, p)
@@ -638,12 +641,18 @@
 
         if si == 0:
             each(queries_step)
+            do_keys()
             each(gradient_step)
-            do_keys()
         elif 2 * si < n:
             each(queries_step)
+            do_keys()
+            for p in range(half):
+                relay_down(si, 1, 1, p)
             hop(si, si, True).start()
+        elif si < last:
             do_keys()
+            hop(si, si, False).start()
+            each(queries_step)
         else:
             do_keys()
             each(queries_step)
@@ -692,11 +701,12 @@
         if si == 0:
             do_values()
             x_over()
+            w_middle(si)
+            w_relay(si, 1)
             do_key_gradients()
             value_sums()
             x_last()
-            w_middle(si)
-            w_relay(si, 1)
+            w_relay(si, 2)
         elif si == last:
             do_values()
             x_over()
@@ -710,25 +720,28 @@
             do_values()
             x_over()
             w_middle(si)
+            each(gradient_step)
             value_sums()
             w_relay_down(si, 1)
-            each(gradient_step)
             x_last()
             do_key_gradients()
             w_relay(si, 2)
+            chain_first(si, 0, half // 2)
         else:
             value_sums(0, half // 2)
             do_values()
-            value_sums(half // 2, half)
-            hop(si, si, False).start()
+            value_sums(half // 2, half - 1)
+            each(gradient_step, 0, half // 2)
+            value_sums(half - 1, half)
             w_relay_down(si, 1)
             x_over()
             w_middle(si)
             w_relay_up(si, 1)
-            each(gradient_step)
+            each(gradient_step, half // 2, half)
             x_last()
+            do_key_gradients()
+            chain_first(si, 0, half // 2)
             w_relay(si, 2)
-            do_key_gradients()
 
     def chain_down(si, begin, end):
         if si < last:
@@ -744,24 +757,29 @@
         (chain_up if 2 * si < n else chain_down)(si, begin, end)
 
     def chain_rest(si):
-        (chain_down if 2 * si < n else chain_up)(si, 0, half)
+        if si == 0:
+            chain_down(si, 0, half)
+        elif 2 * si >= n:
+            chain_up(si, 0, half)
 
     def fourth(si):
-        if si == 0:
-            w_relay(si, 2)
         w_relay(si, 3)
+        w_last(si)
+
+    def fifth(si):
         for j in w_blocks(si, 1):
             w_middle(j)
 
-    def third(si):
+    def sixth(si):
         for j in w_blocks(si, 2):
             w_middle(j)
+        for j in w_blocks(si, 1):
+            w_last(j)
         for j in w_blocks(si, 3):
             w_middle(j)
+
+    def seventh(si):
         chain_rest(si)
-        w_last(si)
-        for j in w_blocks(si, 1):
-            w_last(j)
         for t in (2, 3):
             for j in w_blocks(si, t):
                 w_last(j)
@@ -782,7 +800,9 @@
 
     def by_device(body):
         for si in range(n):
-            pl.when(s == si)(functools.partial(body, si))
+            @pl.when(s == si)
+            def _():
+                body(si)
 
     barrier = pltpu.get_barrier_semaphore()
     for r in range(1, n):
@@ -823,26 +843,35 @@
     pl.when(inner)(lambda: give(mate, 0, 2))
     sum_ref[1] = weight_part(jnp.where(outer, nearest, outermost))
     pl.when(outer)(lambda: give(nearest, 1, 1))
+    by_device(fourth)
     sum_ref[2] = weight_part(jnp.where(outer, mate, nearest))
     pl.when(outer)(lambda: give(mate, 2, 2))
     sum_ref[3] = weight_part(s)
-    by_device(fourth)
-    by_device(lambda si: chain_first(si, 0, half))
-
-    @pl.when(inner)
-    def _():
-        for k, j in ((0, outermost), (1, nearest)):
-            part_copy(j, k, j).wait_recv()
-            part[j] = (sum_ref[k + 1] + part_in[k].astype(f32)).astype(bf16)
-            part_copy(j, 3, j).start()
-
-    by_device(third)
-
-    arrived(("w", "over"), w_all.at[:4])
-    vg_rows = jnp.concatenate([vg[i] for i in range(8)], axis=1)
-    for j in range(n):
+    by_device(lambda si: chain_first(si, half // 2, half))
+    by_device(fifth)
+
+    def pass_part(k, j):
+        part_copy(j, k, j).wait_recv()
+        part[j] = (sum_ref[k + 1] + part_in[k].astype(f32)).astype(bf16)
+        part_copy(j, 3, j).start()
+
+    def input_part(j):
+        remote(w_all.at[:4, j], w_all.at[:4, j], "w", sem("w over", n) + j, s, partner).wait_recv()
+        vg_rows = jnp.concatenate([vg[i] for i in range(8)], axis=1)
         w_rows = jnp.concatenate([w_all[i, j] for i in range(8)], axis=1)
-        ig_ref[:, j * block : (j + 1) * block] = dot(vg_rows, w_rows, BY_LANES).astype(bf16)
+        columns = pl.ds(pl.multiple_of(j * block, LANES), block)
+        ig_ref[:, columns] = dot(vg_rows, w_rows, BY_LANES).astype(bf16)
+
+    input_part(s)
+    for step, j in enumerate((outermost, nearest)):
+        by_device(lambda si: 0 < 2 * si < n and chain_down(si, step * half // 2, (step + 1) * half // 2))
+        pl.when(inner)(lambda: pass_part(step, j))
+
+    by_device(sixth)
+    input_part(mate)
+    by_device(seventh)
+    input_part(nearest)
+    input_part(outermost)
 
     by_device(finish)
     sent("gate", gate_all.at[:last])
@@ -874,7 +903,7 @@
     length = n * rows
     wide = padded(length)
     bf16, f32 = jnp.bfloat16, jnp.float32
-    copies = 7 * (n - 1) * half + 7 * n + 13
+    copies = 7 * (n - 1) * half + 8 * n + 12
     vmem = pl.BlockSpec(memory_space=pltpu.VMEM)
     hbm = pl.BlockSpec(memory_space=pl.ANY)
     results = (

time: 58.6 us -> 54.9 us (0.937)
  Pallas kernels: 57.8 us -> 54 us
    pallas_call x1, Pallas kernels: 56.6 us -> 52.9 us  [fused(): pl.pallas_call(functools.partial(kernel, n, half), out_shape=tuple((pltpu...]
where the time goes in v3:
time: 54.9 us; the launch traced here: 54.7 us
  Pallas kernels  54 us (98%)
  between operations  0.64 us (1%)
    pallas_call x1, Pallas kernels, fused(): pl.pallas_call(functools.partial(kernel, n, half), out_shape=tuple((pltpu...  52.9 us
    pallas_call x1, Pallas kernels, fused(): pl.pallas_call(put_out, out_shape=results, in_specs=[vmem] * 4, out_specs...  1.11 us

profile of v3, /device:TPU:1, one launch (start us, length us, event | category | flops | bytes accessed | tf_op | source)
XLA Modules:
  0.0 54.7 jit_solution(8517022900425885728)
XLA Ops:
  0.6 52.9 %shard_map.102 = (bf16[136,1024]{1,0:T(8,128)(2,1)S(1)}, bf16[136,1024]{1,0:T(8,128)(2,1)S(1)}, bf16[136,2048]{1,0:T(8,128)(2,1)S(1)}, f32[512,128]{1,0:T(8,128)S(1)}) custom-call(bf16[136,2048]{1,0:T(8,128)(2,1)} %bitcast.9, bf16[136,1024]{1,0:T(8,128)(2,1)} %bitcast.10, bf16[136,1024]{1,0:T(8,128)(2,1)} %bitcast.11, bf16[136,1024]{1,0:T(8,128)(2,1)} %bitcast.12, ...), custom_call_target="tpu_custom_call" | custom-call | tf_op jit(solution)/shard_map/pallas_call | solution.py:915
  53.6 1.1 %shard_map.103 = (bf16[136,1024]{1,0:T(8,128)(2,1)}, bf16[136,1024]{1,0:T(8,128)(2,1)}, bf16[136,2048]{1,0:T(8,128)(2,1)}, f32[512,128]{1,0:T(8,128)}) custom-call(bf16[136,1024]{1,0:T(8,128)(2,1)S(1)} %get-tuple-element.12.refs_0_, bf16[136,1024]{1,0:T(8,128)(2,1)S(1)} %get-tuple-element.13.refs_1_, bf16[136,2048]{1,0:T(8,128)(2,1)S(1)} %get-tuple-element.14.refs_2_, ...), custom_call_target="tpu_custom_call" | custom-call | tf_op jit(solution)/shard_map/pallas_call | solution.py:951

commit v4 on v3

--- a/solution.py
+++ b/solution.py
@@ -538,9 +538,11 @@
         upper = 2 * si >= n
         relay(si, 0, 1)
         send_own(si, not upper, 0, half)
+        early = 0 if upper else half // 2
+        send_own(si, upper, 0, early)
         for t in range(2, n):
             relay(si, 0, t)
-        send_own(si, upper, 0, half)
+        send_own(si, upper, early, half)
 
     def w_relay_up(si, t):
         if si - t >= 0:
@@ -645,8 +647,10 @@
             each(gradient_step)
         elif 2 * si < n:
             each(queries_step)
+            for p in range(half // 2):
+                relay_down(si, 1, 1, p)
             do_keys()
-            for p in range(half):
+            for p in range(half // 2, half):
                 relay_down(si, 1, 1, p)
             hop(si, si, True).start()
         elif si < last:
@@ -661,7 +665,6 @@
             relay(si, 1, t)
         if 0 < si < last:
             if 2 * si < n:
-                hop(si, si, False).start()
                 w_relay_up(si, 1)
             else:
                 hop(si, si, True).start()
@@ -702,22 +705,23 @@
             do_values()
             x_over()
             w_middle(si)
+            do_key_gradients()
             w_relay(si, 1)
-            do_key_gradients()
+            x_last()
             value_sums()
-            x_last()
             w_relay(si, 2)
         elif si == last:
             do_values()
             x_over()
             w_middle(si)
             each(gradient_step)
+            w_relay(si, 1)
             x_last()
-            w_relay(si, 1)
             do_key_gradients()
             w_relay(si, 2)
         elif 2 * si < n:
             do_values()
+            hop(si, si, False).start()
             x_over()
             w_middle(si)
             each(gradient_step)
@@ -739,8 +743,8 @@
             w_relay_up(si, 1)
             each(gradient_step, half // 2, half)
             x_last()
+            chain_first(si, 0, half // 2)
             do_key_gradients()
-            chain_first(si, 0, half // 2)
             w_relay(si, 2)
 
     def chain_down(si, begin, end):
@@ -756,11 +760,12 @@
     def chain_first(si, begin, end):
         (chain_up if 2 * si < n else chain_down)(si, begin, end)
 
+    def chain_other(si, begin, end):
+        (chain_down if 2 * si < n else chain_up)(si, begin, end)
+
     def chain_rest(si):
-        if si == 0:
-            chain_down(si, 0, half)
-        elif 2 * si >= n:
-            chain_up(si, 0, half)
+        if si in (0, last):
+            chain_other(si, 0, half)
 
     def fourth(si):
         w_relay(si, 3)
@@ -779,7 +784,6 @@
             w_middle(j)
 
     def seventh(si):
-        chain_rest(si)
         for t in (2, 3):
             for j in w_blocks(si, t):
                 w_last(j)
@@ -843,10 +847,11 @@
     pl.when(inner)(lambda: give(mate, 0, 2))
     sum_ref[1] = weight_part(jnp.where(outer, nearest, outermost))
     pl.when(outer)(lambda: give(nearest, 1, 1))
-    by_device(fourth)
+    pl.when(s == 0)(lambda: fourth(0))
     sum_ref[2] = weight_part(jnp.where(outer, mate, nearest))
     pl.when(outer)(lambda: give(mate, 2, 2))
     sum_ref[3] = weight_part(s)
+    by_device(lambda si: si > 0 and fourth(si))
     by_device(lambda si: chain_first(si, half // 2, half))
     by_device(fifth)
 
@@ -864,7 +869,7 @@
 
     input_part(s)
     for step, j in enumerate((outermost, nearest)):
-        by_device(lambda si: 0 < 2 * si < n and chain_down(si, step * half // 2, (step + 1) * half // 2))
+        by_device(lambda si: 0 < si < last and chain_other(si, step * half // 2, (step + 1) * half // 2))
         pl.when(inner)(lambda: pass_part(step, j))
 
     by_device(sixth)
@@ -872,6 +877,7 @@
     by_device(seventh)
     input_part(nearest)
     input_part(outermost)
+    by_device(chain_rest)
 
     by_device(finish)
     sent("gate", gate_all.at[:last])

time: 54.9 us -> 54.4 us (level)
  no operation moved by 1% of the time
where the time goes in v4:
time: 54.4 us; the launch traced here: 54.1 us
  Pallas kernels  53.5 us (98%)
  between operations  0.64 us (1%)
    pallas_call x1, Pallas kernels, fused(): pl.pallas_call(functools.partial(kernel, n, half), out_shape=tuple((pltpu...  52.4 us
    pallas_call x1, Pallas kernels, fused(): pl.pallas_call(put_out, out_shape=results, in_specs=[vmem] * 4, out_specs...  1.11 us

profile of v4, /device:TPU:1, one launch (start us, length us, event | category | flops | bytes accessed | tf_op | source)
XLA Modules:
  0.0 54.1 jit_solution(9071292734901715311)
XLA Ops:
  0.6 52.4 %shard_map.102 = (bf16[136,1024]{1,0:T(8,128)(2,1)S(1)}, bf16[136,1024]{1,0:T(8,128)(2,1)S(1)}, bf16[136,2048]{1,0:T(8,128)(2,1)S(1)}, f32[512,128]{1,0:T(8,128)S(1)}) custom-call(bf16[136,2048]{1,0:T(8,128)(2,1)} %bitcast.9, bf16[136,1024]{1,0:T(8,128)(2,1)} %bitcast.10, bf16[136,1024]{1,0:T(8,128)(2,1)} %bitcast.11, bf16[136,1024]{1,0:T(8,128)(2,1)} %bitcast.12, ...), custom_call_target="tpu_custom_call" | custom-call | tf_op jit(solution)/shard_map/pallas_call | solution.py:921
  53.0 1.1 %shard_map.103 = (bf16[136,1024]{1,0:T(8,128)(2,1)}, bf16[136,1024]{1,0:T(8,128)(2,1)}, bf16[136,2048]{1,0:T(8,128)(2,1)}, f32[512,128]{1,0:T(8,128)}) custom-call(bf16[136,1024]{1,0:T(8,128)(2,1)S(1)} %get-tuple-element.12.refs_0_, bf16[136,1024]{1,0:T(8,128)(2,1)S(1)} %get-tuple-element.13.refs_1_, bf16[136,2048]{1,0:T(8,128)(2,1)S(1)} %get-tuple-element.14.refs_2_, ...), custom_call_target="tpu_custom_call" | custom-call | tf_op jit(solution)/shard_map/pallas_call | solution.py:957

commit v5 on v4

--- a/solution.py
+++ b/solution.py
@@ -248,11 +248,11 @@
         remote(qg_in.at[a, p, last - b], qg_in.at[a, p, last - b], "down", i, (s + 1) % n, d).wait_recv()
 
     def down_sum(c, b, p):
-        i = sem(("down sum", c, b), half) + p
+        i = sem(("down sum", c, b * (1 - c)), half) + p
         return remote(down_out.at[c, p, b], down_in.at[c, p, b], "down sum", i, (s + n - 1) % n, d)
 
     def up_sum(j, p):
-        i = sem(("up sum", j), half) + p
+        i = sem("up sum", half) + p
         return remote(up_out.at[p, j], up_in.at[p, j], "up sum", i, (s + 1) % n, d)
 
     def gate_copy(sender, to):
@@ -478,10 +478,14 @@
         return dq * scale
 
     def pass_down(si, c, p, total):
+        if c == 1 and si < last:
+            held = down_in.at[c, p, : si + 1]
+            remote(held, held, "up", sem(("down sum", c, 0), half) + p, s, partner).wait_recv()
         for b in range(si + 1):
             value = total[rows * b : rows * (b + 1)]
             if si < last:
-                down_sum(c, b, p).wait_recv()
+                if c == 0:
+                    down_sum(c, b, p).wait_recv()
                 value = value + down_in[c, p, b].astype(f32)
             value = value.astype(bf16)
             if b < si:
@@ -494,10 +498,12 @@
                 kg_ref[:, lanes(p)] = value
 
     def pass_up(si, p, total):
+        if si > 0:
+            held = up_in.at[p, : n - si]
+            remote(held, held, "up", sem("up sum", half) + p, s, partner).wait_recv()
         for j in range(n - si):
             value = total[rows * j : rows * (j + 1)]
             if si > 0:
-                up_sum(j, p).wait_recv()
                 value = value + up_in[p, j].astype(f32)
             value = value.astype(bf16)
             if j < last - si:
@@ -670,6 +676,8 @@
                 hop(si, si, True).start()
         x_all[d] = in_ref[...]
         w_all[d, si] = w_ref[...]
+        if si in (0, last):
+            w_middle(si)
 
         def value_step(p):
             if si == 0:
@@ -704,7 +712,6 @@
         if si == 0:
             do_values()
             x_over()
-            w_middle(si)
             do_key_gradients()
             w_relay(si, 1)
             x_last()
@@ -713,7 +720,6 @@
         elif si == last:
             do_values()
             x_over()
-            w_middle(si)
             each(gradient_step)
             w_relay(si, 1)
             x_last()
@@ -909,7 +915,7 @@
     length = n * rows
     wide = padded(length)
     bf16, f32 = jnp.bfloat16, jnp.float32
-    copies = 7 * (n - 1) * half + 8 * n + 12
+    copies = 5 * (n - 1) * half + 2 * half + 8 * n + 12
     vmem = pl.BlockSpec(memory_space=pltpu.VMEM)
     hbm = pl.BlockSpec(memory_space=pl.ANY)
     results = (

time: 54.4 us -> 54.2 us (level)
  no operation moved by 1% of the time
where the time goes in v5:
time: 54.2 us; the launch traced here: 54 us
  Pallas kernels  53.4 us (99%)
  between operations  0.64 us (1%)
    pallas_call x1, Pallas kernels, fused(): pl.pallas_call(functools.partial(kernel, n, half), out_shape=tuple((pltpu...  52.3 us
    pallas_call x1, Pallas kernels, fused(): pl.pallas_call(put_out, out_shape=results, in_specs=[vmem] * 4, out_specs...  1.11 us

profile of v5, /device:TPU:1, one launch (start us, length us, event | category | flops | bytes accessed | tf_op | source)
XLA Modules:
  0.0 54.0 jit_solution(7036545410273793832)
XLA Ops:
  0.6 52.3 %shard_map.102 = (bf16[136,1024]{1,0:T(8,128)(2,1)S(1)}, bf16[136,1024]{1,0:T(8,128)(2,1)S(1)}, bf16[136,2048]{1,0:T(8,128)(2,1)S(1)}, f32[512,128]{1,0:T(8,128)S(1)}) custom-call(bf16[136,2048]{1,0:T(8,128)(2,1)} %bitcast.9, bf16[136,1024]{1,0:T(8,128)(2,1)} %bitcast.10, bf16[136,1024]{1,0:T(8,128)(2,1)} %bitcast.11, bf16[136,1024]{1,0:T(8,128)(2,1)} %bitcast.12, ...), custom_call_target="tpu_custom_call" | custom-call | tf_op jit(solution)/shard_map/pallas_call | solution.py:927
  52.9 1.1 %shard_map.103 = (bf16[136,1024]{1,0:T(8,128)(2,1)}, bf16[136,1024]{1,0:T(8,128)(2,1)}, bf16[136,2048]{1,0:T(8,128)(2,1)}, f32[512,128]{1,0:T(8,128)}) custom-call(bf16[136,1024]{1,0:T(8,128)(2,1)S(1)} %get-tuple-element.12.refs_0_, bf16[136,1024]{1,0:T(8,128)(2,1)S(1)} %get-tuple-element.13.refs_1_, bf16[136,2048]{1,0:T(8,128)(2,1)S(1)} %get-tuple-element.14.refs_2_, ...), custom_call_target="tpu_custom_call" | custom-call | tf_op jit(solution)/shard_map/pallas_call | solution.py:963
